TPU v7x, 512 devices: a whole 4x8x8 slice. The times are simulated.
512 devices in a mesh: ep: 32 (over z, x), tp: 16 (over y, core).
Axes of the slice: x: 4, y: 8, z: 8, core: 2. Of those that a mesh axis runs over, the one named last changes fastest.
Arguments:
- x_mix: bfloat16 [8192, 2048], P('ep'), may hold values from -6 to 6
- mix_gain: float32 [2048], replicated, may hold values from 0.1 to 1.9
- w_query: bfloat16 [2048, 2048], P(None, 'tp'), may hold values from -0.125 to 0.125
- w_key: bfloat16 [2048, 2048], P(None, 'tp'), may hold values from -0.125 to 0.125
- w_value: bfloat16 [2048, 2048], P(None, 'tp'), may hold values from -0.125 to 0.125
- query_gain: float32 [64], replicated, may hold values from 1 to 1.8
- key_gain: float32 [64], replicated, may hold values from 1 to 1.8
- mix_lambda: float32 [16], P('tp'), may hold values from 0.3 to 0.8
- head_gain: float32 [128], replicated, may hold values from 0.1 to 1.9
- w_mix_out: bfloat16 [2048, 2048], P(None, 'tp'), may hold values from -0.125 to 0.125
- x_exp: bfloat16 [4096, 2048], P('ep'), may hold values from -6 to 6
- exp_gain: float32 [2048], replicated, may hold values from 0.1 to 1.9
- routes: int32 [4096, 4], P('ep'), may hold values from 0 to 31, all different within a row; in each aligned block of 128 rows (0 to 127, 128 to 255, ...) at most 24 rows name the same one
- route_weight: float32 [4096, 4], P('ep'), may hold values from 0.1 to 1
- w_gate: bfloat16 [32, 2048, 2048], P('ep', None, 'tp'), may hold values from -0.375 to 0.375
- w_up: bfloat16 [32, 2048, 2048], P('ep', None, 'tp'), may hold values from -0.375 to 0.375
- w_down: bfloat16 [32, 2048, 2048], P('ep', None, 'tp'), may hold values from -0.03125 to 0.03125
Outputs:
- attn_out: bfloat16 [8192, 2048], P('ep', 'tp')
- moe_out: bfloat16 [4096, 2048], P('ep', 'tp')
Inputs may be any that keep to these rules, and one draw needn't show every extreme that they name: `routes`: each row names 4 different experts. In each aligned block of 128 rows (the rows of one index of ep), no expert is named by more than 24 rows, a bound that some block reaches.
All inputs are finite; a program needn't handle non-finite values.
Results may differ from a plain program's by a relative error of at most 0.011.
Values may be sent and summed in bfloat16 or wider, within the bound.
No kernel may reach another device: no remote copies, remote signals or barrier semaphores. Data moves between devices by JAX's collectives and lax.ppermute only.
A program may use at most 128 MiB of HBM per device.

v0:
```python
import jax
import jax.numpy as jnp
from jax import lax
from jax.sharding import Mesh
from jax.sharding import PartitionSpec as P

TP = ("tp_0", "tp_1")


def in_one_piece(arrays, axis, dim, along):
    widths = [a.shape[along] for a in arrays]
    both = jnp.concatenate(arrays, axis=along)
    out = lax.all_gather(both, axis, axis=dim, tiled=True)
    return tuple(jnp.split(out, [sum(widths[:k]) for k in range(1, len(widths))], axis=along))


def whole_of(x, axes, dim):
    out = x
    for number in range(len(axes) - 1, -1, -1):
        out = lax.all_gather(out, axes[number], axis=dim, tiled=True)
    return out


def rms_rows(matrix, gain, epsilon):
    wide = matrix.astype(jnp.float32)
    return wide * lax.rsqrt(jnp.mean(wide * wide, axis=-1, keepdims=True) + epsilon) * gain


def slot_ids(chosen_rows, experts, capacity):
    flat_ids = chosen_rows.reshape(-1)
    onehot = (flat_ids[:, None] == lax.iota(jnp.int32, experts)[None, :]).astype(jnp.int32)
    before = jnp.cumsum(onehot, axis=0) - onehot
    position = jnp.sum(before * onehot, axis=1)
    return flat_ids * capacity + position


def attend(
    x_mix, mix_gain, w_query, w_key, w_value, query_gain, key_gain, mix_lambda, head_gain, w_mix_out
):
    row_count = x_mix.shape[0]
    head_size = query_gain.shape[0]
    head_count = w_query.shape[1] // (2 * head_size)
    normed = rms_rows(x_mix, mix_gain, 1e-05).astype(jnp.bfloat16)
    queries = jnp.dot(normed, w_query, preferred_element_type=jnp.float32).reshape(
        row_count, head_count, 2, head_size
    )
    queries = (rms_rows(queries, query_gain, 1e-06) * head_size ** (-0.5)).astype(jnp.bfloat16)
    key_rows = jnp.dot(normed, w_key, preferred_element_type=jnp.float32).reshape(
        row_count, head_count, 2, head_size
    )
    key_rows = (
        rms_rows(key_rows, key_gain, 1e-06)
        .astype(jnp.bfloat16)
        .reshape(row_count, head_count * 2 * head_size)
    )
    values = jnp.dot(normed, w_value, preferred_element_type=jnp.float32).astype(jnp.bfloat16)
    query_pos = lax.axis_index("ep") * row_count + lax.iota(jnp.int32, row_count)
    key_piece, value_piece = in_one_piece((key_rows, values), "ep", 0, 1)
    piece_rows = key_piece.shape[0]
    key_piece = key_piece.reshape(piece_rows, head_count, 2, head_size)
    value_piece = value_piece.reshape(piece_rows, head_count, 2 * head_size)
    scores = jnp.einsum("qhcd,khcd->cqhk", queries, key_piece, preferred_element_type=jnp.float32)
    key_pos = lax.iota(jnp.int32, piece_rows)
    visible = key_pos[None, :] <= query_pos[:, None]
    weights_exp = jnp.where(visible[None, :, None, :], jnp.exp(scores), 0.0)
    denominator = jnp.sum(weights_exp, axis=-1)
    numerator = jnp.einsum(
        "cqhk,khd->cqhd",
        weights_exp.astype(jnp.bfloat16),
        value_piece,
        preferred_element_type=jnp.float32,
    )
    numerator, denominator = (numerator, denominator)
    head_mix = (
        numerator[0] / denominator[0][..., None]
        - mix_lambda[None, :, None] * numerator[1] / denominator[1][..., None]
    )
    head_rows = (rms_rows(head_mix, head_gain, 1e-05) * 0.8).astype(jnp.bfloat16)
    head_rows = head_rows.reshape(row_count, head_count * 2 * head_size)
    projected = jnp.dot(whole_of(head_rows, TP, 1), w_mix_out, preferred_element_type=jnp.float32)
    return projected.astype(jnp.bfloat16)


def route_experts(x_exp, exp_gain, routes, route_weight, w_gate, w_up, w_down):
    row_count = x_exp.shape[0]
    top_count = routes.shape[1]
    model_width = x_exp.shape[1]
    experts = lax.axis_size("ep")
    capacity = 3 * row_count * top_count // (2 * experts)
    gate_local = w_gate[0]
    up_local = w_up[0]
    down_local = w_down[0]
    local_width = down_local.shape[1]
    normed = rms_rows(x_exp, exp_gain, 1e-05).astype(jnp.bfloat16)
    slot_index = slot_ids(routes, experts, capacity)
    pair_rows = lax.iota(jnp.int32, row_count * top_count) // top_count
    source = jnp.zeros((experts * capacity,), jnp.int32).at[slot_index].set(pair_rows)
    filled = jnp.zeros((experts * capacity,), jnp.bool_).at[slot_index].set(True)
    picked_rows = jnp.where(filled[:, None], normed[source], jnp.zeros((), jnp.bfloat16))
    outgoing = picked_rows.reshape(experts, capacity, model_width)
    incoming = lax.all_to_all(outgoing, "ep", split_axis=0, concat_axis=0, tiled=True)
    item_count = incoming.shape[1]
    flat_rows = incoming.reshape(-1, model_width)
    gate_pre = jnp.dot(flat_rows, gate_local, preferred_element_type=jnp.float32)
    up_pre = jnp.dot(flat_rows, up_local, preferred_element_type=jnp.float32)
    expert_gate_pre = gate_pre
    expert_up_pre = up_pre
    expert_gate_pre = jnp.minimum(expert_gate_pre, 7.0)
    expert_up_pre = jnp.clip(expert_up_pre, -7.0, 7.0)
    hidden = (
        expert_gate_pre * jax.nn.sigmoid(1.702 * expert_gate_pre) * (expert_up_pre + 1.0)
    ).astype(jnp.bfloat16)
    result = jnp.dot(
        lax.all_gather(hidden, TP, axis=1, tiled=True),
        down_local,
        preferred_element_type=jnp.float32,
    )
    result = result.astype(jnp.bfloat16).reshape(experts, item_count, local_width)
    returned = lax.all_to_all(result, "ep", split_axis=0, concat_axis=0, tiled=True)
    picked = returned.reshape(experts * capacity, local_width)[slot_index]
    picked = picked.reshape(row_count, top_count, local_width).astype(jnp.float32)
    combined = jnp.sum(picked * route_weight[:, :, None], axis=1)
    return combined.astype(jnp.bfloat16)


def body(
    x_mix,
    mix_gain,
    w_query,
    w_key,
    w_value,
    query_gain,
    key_gain,
    mix_lambda,
    head_gain,
    w_mix_out,
    x_exp,
    exp_gain,
    routes,
    route_weight,
    w_gate,
    w_up,
    w_down,
):
    attn_out = attend(
        x_mix,
        mix_gain,
        w_query,
        w_key,
        w_value,
        query_gain,
        key_gain,
        mix_lambda,
        head_gain,
        w_mix_out,
    )
    moe_out = route_experts(x_exp, exp_gain, routes, route_weight, w_gate, w_up, w_down)
    return (attn_out, moe_out)


def solution(mesh):
    finer = Mesh(mesh.devices.reshape(mesh.shape["ep"], 8, 2), ("ep", "tp_0", "tp_1"))
    placed = (
        P("ep", None),
        P(),
        P(None, TP),
        P(None, TP),
        P(None, TP),
        P(),
        P(),
        P(TP),
        P(),
        P(None, TP),
        P("ep", None),
        P(),
        P("ep", None),
        P("ep", None),
        P("ep", None, TP),
        P("ep", None, TP),
        P("ep", None, TP),
    )
    return jax.shard_map(
        body, mesh=finer, in_specs=placed, out_specs=(P("ep", TP), P("ep", TP)), check_vma=False
    )
```

profile of v0, /device:TPU:1, one launch (start us, length us, event | category | flops | bytes accessed | tf_op | source)
XLA Modules:
  0.0 237.6 jit_solution(2893565532655223578)
XLA Ops:
  7.3 1.6 fusion.7
  9.0 2.0 bitcast_reduce_fusion.1
  11.1 0.6 convolution_convert_fusion.2
  11.8 0.7 pad_maximum_fusion
  12.5 0.1 copy.25
  12.9 1.2 reduce-window.6
  14.1 0.2 slice_reduce_fusion
  14.7 2.4 %scatter_custom_fusion.1 = s32[768]{0:T(1024)S(1)} fusion(s32[512]{0:T(512)S(1)} %bitcast.130, s32[512]{0:T(512)S(1)} %add_select_fusion, s32[]{:T(128)} %constant.65.clone.1), kind=kCustom, calls=%fused_computation.80 | custom fusion | bytes 3076 | tf_op jit(solution)/shard_map/scatter | solution.py:97
  17.1 0.2 fusion.13
  17.3 2.4 %scatter_custom_fusion = pred[768]{0:T(1024)(128)(4,1)S(1)} fusion(s32[512]{0:T(512)S(1)} %bitcast.131, pred[512]{0:T(512)(128)(4,1)S(1)} %broadcast.237, pred[]{:T(512)} %constant.25.clone.1), kind=kCustom, calls=%fused_computation.85 | custom fusion | bytes 769 | tf_op jit(solution)/shard_map/scatter | solution.py:98
  19.9 0.2 fusion.15
  20.1 4.3 %gather_fusion = bf16[768,2048]{1,0:T(8,128)(2,1)} fusion(bf16[128,2048]{1,0:T(8,128)(2,1)S(1)} %fusion.15, s32[1024]{0:T(1024)S(1)} %pad_clamp_fusion.1), kind=kCustom, calls=%fused_computation | custom fusion | bytes 6294528 | tf_op jit(solution)/shard_map/gather | solution.py:99
  24.4 2.2 broadcast_select_fusion
  26.6 97.3 %all_to_all.10 = bf16[32,24,2048]{2,1,0:T(8,128)(2,1)S(1)} all-to-all(bf16[32,24,2048]{2,1,0:T(8,128)(2,1)S(1)} %broadcast_select_fusion), channel_id=1, replica_groups=mesh['ep'=32,'tp_0'=8,'tp_1'=2] {'ep'}, dimensions={0} | all-to-all | bytes 6291456 | tf_op jit(solution)/shard_map/all_to_all | solution.py:101
  123.9 1.0 convolution_minimum_fusion
  124.9 1.7 fusion.12
  126.6 0.2 all-gather.6.cloned.1.call-start
  127.5 0.6 bitcast_reduce_fusion
  128.1 1.4 iota_compare_fusion
  129.5 10.5 %all-gather.4.cloned.1.call-done = bf16[8192,256]{0,1:T(8,128)(2,1)} async-done(((bf16[256,256]{0,1:T(8,128)(2,1)}), bf16[8192,256]{0,1:T(8,128)(2,1)}) %all-gather.4.cloned.1.call-update) | async-done | bytes 4194320 | tf_op jit(solution)/shard_map/all_gather | solution.py:13
  140.0 1.6 slice-done
  141.6 7.6 %fusion = (f32[2,256]{1,0:T(2,128)S(1)}, f32[2,8192,256]{2,1,0:T(8,128)}) fusion(pred[256,8192]{0,1:T(8,128)(4,1)S(1)} %iota_compare_fusion, bf16[8192,2,64]{0,2,1:T(8,128)(2,1)S(1)} %bitcast.120, f32[256,2,64]{0,2,1:T(8,128)S(1)} %bitcast.134, f32[64]{0:T(128)S(1)} %copy-done.15, f32[256,2]{0,1:T(2,128)S(1)} %add_rsqrt_fusion), kind=kOutput, calls=%fused_computation.5 | convolution fusion | flops 545390080 | bytes 21106944 | tf_op jit(solution)/shard_map/qhcd,khcd->cqhk/dot_general | solution.py:62
  149.2 7.5 %fusion.3 = f32[128,2,256]{2,0,1:T(8,128)S(1)} fusion(f32[2,8192,256]{2,1,0:T(8,128)} %get-tuple-element.9, pred[256,8192]{0,1:T(8,128)(4,1)S(1)} %iota_compare_fusion, bf16[8192,256]{0,1:T(8,128)(2,1)S(1)} %copy-done.1), kind=kOutput, calls=%fused_computation.8 | convolution fusion | flops 1082130432 | bytes 21233664 | tf_op jit(solution)/shard_map/cqhk,khd->cqhd/dot_general | solution.py:67
  156.9 5.1 %all_gather.13 = bf16[256,256]{0,1:T(8,128)(2,1)} all-gather(bf16[256,128]{0,1:T(8,128)(2,1)S(1)} %fusion.28), channel_id=1, replica_groups=mesh['ep'=32,'tp_0'=8,'tp_1'=2] {'tp_1'}, dimensions={1}, use_global_device_ids=true | all-gather | bytes 196608 | tf_op jit(solution)/shard_map/all_gather | solution.py:20
  162.0 28.2 %all-gather.8.cloned.1.call-done = bf16[768,2048]{1,0:T(8,128)(2,1)} async-done(((bf16[768,128]{1,0:T(8,128)(2,1)}), bf16[768,2048]{1,0:T(8,128)(2,1)}) %all-gather.8.cloned.1.call-update) | async-done | bytes 3145744 | tf_op jit(solution)/shard_map/all_gather | solution.py:114
  190.2 3.6 %convolution_convert_fusion = bf16[768,128]{1,0:T(8,128)(2,1)} fusion(bf16[768,2048]{1,0:T(8,128)(2,1)} %all-gather.8.cloned.1.call-done, bf16[1,2048,128]{2,1,0:T(8,128)(2,1)S(1)} %copy-done.12), kind=kOutput, calls=%fused_computation.25 | convolution fusion | flops 402751488 | bytes 3866624 | tf_op jit(solution)/shard_map/dot_general | solution.py:113
  193.8 9.0 %all-to-all-start.1 = ((bf16[32,24,128]{2,1,0:T(8,128)(2,1)}), bf16[32,24,128]{2,1,0:T(8,128)(2,1)S(1)}, u32[]{:S(2)}, u32[]{:S(2)}) async-start(bf16[32,24,128]{2,1,0:T(8,128)(2,1)} %bitcast.28), calls=%async_computation.1 | async-start | bytes 393216 | tf_op jit(solution)/shard_map/all_to_all | solution.py:119
  202.8 0.1 copy.28
  202.9 23.6 %all-gather.6.cloned.1.call-done = bf16[256,2048]{0,1:T(8,128)(2,1)} async-done(((bf16[256,256]{0,1:T(8,128)(2,1)}), bf16[256,2048]{0,1:T(8,128)(2,1)}) %all-gather.6.cloned.1.call-update) | async-done | bytes 1048592 | tf_op jit(solution)/shard_map/all_gather | solution.py:20
  226.5 2.3 convolution_convert_fusion.1
  228.9 1.3 gather_fusion.1
  230.2 0.9 fusion.19
  (67 shorter events, 1.4 us)
Async XLA Ops:
  7.2 116.7 %copy-start = (bf16[1,2048,128]{2,1,0:T(8,128)(2,1)S(1)}, bf16[1,2048,128]{2,1,0:T(8,128)(2,1)}, u32[]{:S(2)}) copy-start(bf16[1,2048,128]{2,1,0:T(8,128)(2,1)} %param.31) | copy-start | bytes 1572868
  7.2 3.9 %copy-start.3 = (bf16[256,2048]{1,0:T(8,128)(2,1)S(1)}, bf16[256,2048]{1,0:T(8,128)(2,1)}, u32[]{:S(2)}) copy-start(bf16[256,2048]{1,0:T(8,128)(2,1)} %param.17) | copy-start | bytes 3145732
  7.2 3.9 %copy-start.13 = (f32[2048]{0:T(1024)S(1)}, f32[2048]{0:T(1024)}, u32[]{:S(2)}) copy-start(f32[2048]{0:T(1024)} %param.18) | copy-start | bytes 24580
  7.2 3.8 %copy-start.14 = (f32[64]{0:T(128)S(1)}, f32[64]{0:T(128)}, u32[]{:S(2)}) copy-start(f32[64]{0:T(128)} %param.23) | copy-start | bytes 772
  7.2 3.9 %copy-start.9 = (bf16[2048,128]{1,0:T(8,128)(2,1)S(1)}, bf16[2048,128]{1,0:T(8,128)(2,1)}, u32[]{:S(2)}) copy-start(bf16[2048,128]{1,0:T(8,128)(2,1)} %param.21) | copy-start | bytes 1572868
  7.2 5.3 %copy-start.6 = (s32[128,4]{0,1:T(4,128)S(1)}, s32[128,4]{0,1:T(4,128)}, u32[]{:S(2)}) copy-start(s32[128,4]{0,1:T(4,128)} %param.29) | copy-start | bytes 6148
  7.2 132.8 %all-gather.4.cloned.1.call-start = ((), (), s32[]{:S(2)}) async-start(), calls=%async_computation.2 | async-start | bytes 4325376 | tf_op jit(solution)/shard_map/all_gather | solution.py:13
  8.9 8.2 %copy-start.2 = (bf16[128,2048]{1,0:T(8,128)(2,1)S(1)}, bf16[128,2048]{1,0:T(8,128)(2,1)}, u32[]{:S(2)}) copy-start(bf16[128,2048]{1,0:T(8,128)(2,1)} %param.27) | copy-start | bytes 1572868
  8.9 11.0 %copy-start.5 = (f32[2048]{0:T(1024)S(1)}, f32[2048]{0:T(1024)}, u32[]{:S(2)}) copy-start(f32[2048]{0:T(1024)} %param.28) | copy-start | bytes 24580
  12.5 177.8 %all-gather.8.cloned.1.call-start = ((), (), s32[]{:S(2)}) async-start(), calls=%async_computation.4 | async-start | bytes 3342336 | tf_op jit(solution)/shard_map/all_gather | solution.py:114
  123.9 1.1 copy-start.10
  124.9 2.6 %copy-start.11 = (bf16[2048,128]{1,0:T(8,128)(2,1)S(1)}, bf16[2048,128]{1,0:T(8,128)(2,1)}, u32[]{:S(2)}) copy-start(bf16[2048,128]{1,0:T(8,128)(2,1)} %param.19) | copy-start | bytes 1572868
  126.6 99.9 %all-gather.6.cloned.1.call-start = ((), (), s32[]{:S(2)}) async-start(), calls=%async_computation.3 | async-start | bytes 1179648 | tf_op jit(solution)/shard_map/all_gather | solution.py:20
  128.1 11.9 %copy-start.15 = (f32[64]{0:T(128)S(1)}, f32[64]{0:T(128)}, u32[]{:S(2)}) copy-start(f32[64]{0:T(128)} %param.22) | copy-start | bytes 772
  140.0 1.6 slice-start
  141.6 7.6 %copy-start.1 = (bf16[8192,256]{0,1:T(8,128)(2,1)S(1)}, bf16[8192,256]{0,1:T(8,128)(2,1)}, u32[]{:S(2)}) copy-start(bf16[8192,256]{0,1:T(8,128)(2,1)} %all-gather.4.cloned.1.call-done) | copy-start | bytes 12582916
  149.2 7.6 %copy-start.8 = (f32[128]{0:T(128)S(1)}, f32[128]{0:T(128)}, u32[]{:S(2)}) copy-start(f32[128]{0:T(128)} %param.25) | copy-start | bytes 1540
  149.2 41.0 %copy-start.12 = (bf16[1,2048,128]{2,1,0:T(8,128)(2,1)S(1)}, bf16[1,2048,128]{2,1,0:T(8,128)(2,1)}, u32[]{:S(2)}) copy-start(bf16[1,2048,128]{2,1,0:T(8,128)(2,1)} %param.33) | copy-start | bytes 1572868
  156.7 46.1 %copy-start.7 = (f32[128,4]{0,1:T(4,128)S(1)}, f32[128,4]{0,1:T(4,128)}, u32[]{:S(2)}) copy-start(f32[128,4]{0,1:T(4,128)} %param.30) | copy-start | bytes 6148
  156.7 69.8 %copy-start.4 = (bf16[2048,128]{1,0:T(8,128)(2,1)S(1)}, bf16[2048,128]{1,0:T(8,128)(2,1)}, u32[]{:S(2)}) copy-start(bf16[2048,128]{1,0:T(8,128)(2,1)} %param.26) | copy-start | bytes 1572868
  193.8 35.0 %all-to-all-start.1 = ((bf16[32,24,128]{2,1,0:T(8,128)(2,1)}), bf16[32,24,128]{2,1,0:T(8,128)(2,1)S(1)}, u32[]{:S(2)}, u32[]{:S(2)}) async-start(bf16[32,24,128]{2,1,0:T(8,128)(2,1)} %bitcast.28), calls=%async_computation.1 | async-start | bytes 393216 | tf_op jit(solution)/shard_map/all_to_all | solution.py:119
Sparse Core Ops, SparseCore 0:
  12.6 127.3 all-gather.3
  142.1 48.1 all-gather.7
  192.3 34.1 all-gather.5
where the time goes:
time: 242 us; the launch traced here: 238 us
  blocking collectives  102 us (42%)
  waiting for transfers between devices  62.3 us (26%)
  matrix products  26.8 us (11%)
  between operations  14.8 us (6%)
  local copies, waits for them, and re-layouts  13.3 us (5%)
  starting transfers between devices  9.28 us (4%)
  other arithmetic  8.72 us (4%)
    all_to_all x1, blocking collectives, route_experts(): lax.all_to_all(outgoing, 'ep', split_axis=0, concat_axis=0, tiled=True)  97.3 us
    all_gather x1, waiting for transfers between devices, route_experts(): lax.all_gather(hidden, TP, axis=1, tiled=True)  28.2 us
    all_gather x1, waiting for transfers between devices, whole_of(): out = lax.all_gather(out, axes[number], axis=dim, tiled=True)  23.6 us
    all_gather x1, waiting for transfers between devices, in_one_piece(): out = lax.all_gather(both, axis, axis=dim, tiled=True)  10.5 us
    all_to_all x1, starting transfers between devices, route_experts(): lax.all_to_all(result, 'ep', split_axis=0, concat_axis=0, tiled=True)  8.98 us
    dot_general x1, matrix products, attend(): jnp.einsum('qhcd,khcd->cqhk', queries, key_piece, preferred_element_type=...  7.57 us
    dot_general x1, matrix products, attend(): jnp.einsum('cqhk,khd->cqhd', weights_exp.astype(jnp.bfloat16), value_piec...  7.46 us
    all_gather x1, blocking collectives, whole_of(): out = lax.all_gather(out, axes[number], axis=dim, tiled=True)  5.15 us
  transfers between devices with their start and end apart: 4, of which 3 were waited for; matrix products, arithmetic and copies ran while one was open for 17% of the time, Pallas kernels for 0%

commit v1 on v0

v1 whole, which is shorter than its diff:
```python
import jax
import jax.numpy as jnp
from jax import lax
from jax.experimental import pallas as pl
from jax.experimental.pallas import tpu as pltpu
from jax.sharding import Mesh
from jax.sharding import PartitionSpec as P

BF = jnp.bfloat16
F32 = jnp.float32
EP = ("z", "x")
TP = ("g", "r", "c")
QUAD = ("r", "c")


def dot(a, b, dims=((1,), (0,))):
    return lax.dot_general(a, b, (dims, ((), ())), preferred_element_type=F32)


def call(kernel, shapes, scratch=(), smem_first=True, count=0):
    specs = [pl.BlockSpec(memory_space=pltpu.VMEM)] * count
    if smem_first:
        specs = [pl.BlockSpec(memory_space=pltpu.SMEM)] + specs
    multiple = isinstance(shapes, (list, tuple))
    out_specs = pl.BlockSpec(memory_space=pltpu.VMEM)
    return pl.pallas_call(
        kernel,
        out_shape=tuple(shapes) if multiple else shapes,
        in_specs=specs,
        out_specs=tuple([out_specs] * len(shapes)) if multiple else out_specs,
        scratch_shapes=list(scratch),
    )


def rms(wide, gain, epsilon):
    scale = lax.rsqrt(jnp.mean(wide * wide, axis=-1, keepdims=True) + epsilon)
    return wide * scale * gain


def expert_tables(routes_ref, experts):
    tokens = routes_ref.shape[1]
    expert = lax.broadcasted_iota(jnp.int32, (experts, tokens), 0)
    named = jnp.zeros((experts, tokens), jnp.bool_)
    for k in range(routes_ref.shape[0]):
        named = named | (routes_ref[k : k + 1, :] == expert)
    earlier = lax.broadcasted_iota(jnp.int32, (tokens, tokens), 0) < lax.broadcasted_iota(
        jnp.int32, (tokens, tokens), 1
    )
    counts = dot(
        jnp.where(named, 1.0, 0.0).astype(BF), jnp.where(earlier, 1.0, 0.0).astype(BF)
    )
    return jnp.where(named, counts, -1.0), expert


def spread(table, times):
    rows, lanes = table.shape
    return jnp.broadcast_to(table[:, None, :], (rows, times, lanes)).reshape(rows * times, lanes)


def dispatch_kernel(place_ref, x_ref, gain_ref, routes_ref, out_ref):
    experts = out_ref.shape[0]
    position, _ = expert_tables(routes_ref, experts)
    tokens, width = x_ref.shape
    chunk = width // 4
    wide = spread(position, 24)
    row = lax.broadcasted_iota(jnp.int32, wide.shape, 0) % 24
    wanted = (row % 6 + 6 * place_ref[0]).astype(F32)
    hit = wide == wanted
    normed = rms(x_ref[...].astype(F32), gain_ref[...], 1e-05).astype(BF)
    total = None
    for part in range(4):
        pick = jnp.where(hit & (row // 6 == part), 1.0, 0.0).astype(BF)
        piece = dot(pick, normed[:, part * chunk : (part + 1) * chunk])
        total = piece if total is None else total + piece
    out_ref[...] = total.astype(BF).reshape(out_ref.shape)


def qkv_kernel(x_ref, gain_ref, wq_ref, wk_ref, wv_ref, qg_ref, kg_ref, q_ref, kv_ref):
    normed = rms(x_ref[...].astype(F32), gain_ref[...], 1e-05).astype(BF)

    def component_norm(wide, gain):
        low = lax.broadcasted_iota(jnp.int32, wide.shape, 1) < 64
        square = wide * wide
        first = jnp.sum(jnp.where(low, square, 0.0), axis=-1, keepdims=True)
        second = jnp.sum(jnp.where(low, 0.0, square), axis=-1, keepdims=True)
        scale = jnp.where(
            low, lax.rsqrt(first / 64 + 1e-06), lax.rsqrt(second / 64 + 1e-06)
        )
        return wide * scale * gain

    q = (component_norm(dot(normed, wq_ref[...]), qg_ref[...]) * 0.125).astype(BF)
    k = component_norm(dot(normed, wk_ref[...]), kg_ref[...]).astype(BF)
    v = dot(normed, wv_ref[...]).astype(BF)
    for n in range(q_ref.shape[0]):
        q_ref[n] = q
    for n in range(kv_ref.shape[0]):
        kv_ref[n, :, 0:128] = k
        kv_ref[n, :, 128:256] = v


def flash_kernel(place_ref, q_ref, kv_ref, out_ref, total_ref):
    z = place_ref[0]
    x = place_ref[1]
    groups, rows = q_ref.shape[0], q_ref.shape[1]
    keys = kv_ref.shape[1]
    total_ref[...] = jnp.zeros_like(total_ref)
    ones = jnp.ones((2 * keys, 128), BF)

    def step(pair, masked):
        kv = kv_ref[pl.ds(2 * pair, 2)].reshape(2 * keys, 256)
        value = jnp.concatenate([kv[:, 128:256], ones], axis=1)
        for group in range(groups):
            for comp in range(2):
                lanes = slice(64 * comp, 64 * comp + 64)
                scores = dot(q_ref[group, :, lanes], kv[:, lanes], ((1,), (1,)))
                weight = jnp.exp(scores)
                if masked:
                    col = lax.broadcasted_iota(jnp.int32, scores.shape, 1)
                    block = 2 * pair + col // keys
                    key_pos = 1024 * block + 256 * x + col % keys
                    query_pos = (
                        1024 * z
                        + rows * group
                        + lax.broadcasted_iota(jnp.int32, scores.shape, 0)
                    )
                    weight = jnp.where(key_pos <= query_pos, weight, 0.0)
                total_ref[comp, group] += dot(weight.astype(BF), value)

    def free_step(pair, carry):
        step(pair, False)
        return carry

    lax.fori_loop(0, z // 2, free_step, 0)
    step(z // 2, True)
    lane = lax.broadcasted_iota(jnp.int32, (rows, 128), 1)
    for group in range(groups):
        first = total_ref[0, group, :, 128:256]
        second = total_ref[1, group, :, 128:256]
        first_high = first.astype(BF).astype(F32)
        second_high = second.astype(BF).astype(F32)
        sums = jnp.where(
            lane < 32,
            first_high,
            jnp.where(
                lane < 64,
                first - first_high,
                jnp.where(lane < 96, second_high, second - second_high),
            ),
        )
        out_ref[group, :, 0:128] = total_ref[0, group, :, 0:128].astype(BF)
        out_ref[group, :, 128:256] = total_ref[1, group, :, 0:128].astype(BF)
        out_ref[group, :, 256:384] = sums.astype(BF)


def mix_kernel(lam_ref, part_ref, gain_ref, out_ref):
    total = part_ref[0].astype(F32)
    for n in range(1, part_ref.shape[0]):
        total = total + part_ref[n].astype(F32)
    sums = total[:, 256:384]
    first = sums[:, 0:1] + sums[:, 32:33]
    second = sums[:, 64:65] + sums[:, 96:97]
    mix = total[:, 0:128] / first - lam_ref[0] * total[:, 128:256] / second
    rows = (rms(mix, gain_ref[...], 1e-05) * 0.8).astype(BF)
    half = rows.shape[0] // 2
    for n in range(out_ref.shape[0] // 2):
        out_ref[2 * n] = rows[0:half]
        out_ref[2 * n + 1] = rows[half:]


def project_kernel(rows_ref, own_ref, other_ref, own_out, other_out):
    rows = jnp.concatenate([rows_ref[n] for n in range(rows_ref.shape[0])], axis=1)
    own_out[...] = dot(rows, own_ref[...]).astype(BF)
    other_out[...] = dot(rows, other_ref[...]).astype(BF)


def hidden_kernel(place_ref, in_ref, *refs):
    weights, out_ref = refs[:-1], refs[-1]
    place = place_ref[0]
    sources = in_ref.shape[0]
    flat = in_ref[...].reshape(sources * 24, in_ref.shape[2])
    count = sources * 6
    line = lax.broadcasted_iota(jnp.int32, (count, sources * 24), 0)
    slot = lax.broadcasted_iota(jnp.int32, (count, sources * 24), 1)
    base = (line // 6) * 24 + line % 6
    pieces = []
    for part in range(4):
        pick = jnp.where(slot == base + 6 * part, 1.0, 0.0).astype(BF)
        pieces.append(dot(pick, flat).astype(BF))
    rows = jnp.concatenate(pieces, axis=1)
    for n in range(4):
        gate = jnp.minimum(dot(rows, weights[2 * n][0]), 7.0)
        up = jnp.clip(dot(rows, weights[2 * n + 1][0]), -7.0, 7.0)
        hidden = (gate * jax.nn.sigmoid(1.702 * gate) * (up + 1.0)).astype(BF)
        for peer in range(out_ref.shape[0]):
            out_ref[peer, place ^ n] = hidden


def down_kernel(place_ref, hidden_ref, *refs):
    weights, out_ref = refs[:-1], refs[-1]
    place = place_ref[0]
    rows = jnp.concatenate(
        [hidden_ref[g, a] for g in range(hidden_ref.shape[0]) for a in range(4)], axis=1
    )
    count = rows.shape[0]
    sources = count // 6
    wide = lax.broadcasted_iota(jnp.int32, (sources * 8, count), 0)
    line = lax.broadcasted_iota(jnp.int32, (sources * 8, count), 1)
    hit = ((wide // 8) * 6 + wide % 8 == line) & (wide % 8 < 6)
    pick = jnp.where(hit, 1.0, 0.0).astype(BF)
    for n in range(4):
        result = dot(rows, weights[n][0]).astype(BF)
        result = dot(pick, result).astype(BF)
        out_ref[:, place ^ n] = result.reshape(sources, 8, result.shape[1])


def combine_kernel(routes_ref, weight_ref, rows_ref, out_ref):
    experts = rows_ref.shape[0] // 4
    position, expert = expert_tables(routes_ref, experts)
    weight = jnp.zeros(position.shape, F32)
    for k in range(routes_ref.shape[0]):
        weight = weight + jnp.where(routes_ref[k : k + 1, :] == expert, weight_ref[k : k + 1, :], 0.0)
    wide = spread(position, 32)
    row = lax.broadcasted_iota(jnp.int32, wide.shape, 0) % 32
    slot = jnp.where(row % 8 < 6, (row // 8) * 6 + row % 8, 1000).astype(F32)
    table = jnp.where(wide == slot, spread(weight, 32), 0.0)
    high = table.astype(BF)
    low = (table - high.astype(F32)).astype(BF)
    rows = rows_ref[...].reshape(experts * 32, rows_ref.shape[2])
    dims = ((0,), (0,))
    out_ref[...] = (dot(high, rows, dims) + dot(low, rows, dims)).astype(BF)


def exchange(a, axes):
    return lax.all_to_all(a, axes, 0, 0, tiled=True)


def swap(a, axes, size, flip):
    return lax.ppermute(a, axes, [(n, n ^ flip) for n in range(size)])


def body(
    x_mix,
    mix_gain,
    w_query,
    w_key,
    w_value,
    query_gain,
    key_gain,
    mix_lambda,
    head_gain,
    w_mix_out,
    x_exp,
    exp_gain,
    routes,
    route_weight,
    w_gate,
    w_up,
    w_down,
):
    core = lax.axis_index("c")
    place = (lax.axis_index("r") * 2 + core).astype(jnp.int32)[None]
    where = jnp.stack([lax.axis_index("z"), lax.axis_index("x")]).astype(jnp.int32)
    shape = jax.ShapeDtypeStruct
    rows_a = x_mix.shape[0]
    rows_b = x_exp.shape[0]

    own = jnp.concatenate([w_gate, w_up, w_down], axis=0)
    far = swap(own, "r", 2, 1)
    near = swap(own, "c", 2, 1)
    cross = swap(far, "c", 2, 1)
    other_out = swap(w_mix_out, "c", 2, 1)
    quad = (own, near, far, cross)

    routes_t = routes.T
    outgoing = call(dispatch_kernel, shape((32, 24, 512), BF), count=3)(
        place, x_exp, exp_gain[None], routes_t
    )
    incoming = exchange(outgoing, EP)

    two = lambda gain: jnp.concatenate([gain, gain])[None]
    q_send, kv_send = call(
        qkv_kernel,
        (shape((4, rows_a, 128), BF), shape((8, rows_a, 256), BF)),
        smem_first=False,
        count=7,
    )(x_mix, mix_gain[None], w_query, w_key, w_value, two(query_gain), two(key_gain))
    q_all = exchange(q_send, "x")
    kv_all = exchange(kv_send, "z")

    def weight_specs(names):
        return [pl.BlockSpec((1, 2048, 128), lambda n, m=m: (m, 0, 0)) for _ in range(4) for m in names]

    full = lambda s: pl.BlockSpec(s, lambda n: (0,) * len(s))
    hidden = pl.pallas_call(
        hidden_kernel,
        grid=(1,),
        out_shape=shape((4, 4, 192, 128), BF),
        in_specs=[pl.BlockSpec(memory_space=pltpu.SMEM), full((32, 24, 512))] + weight_specs((0, 1)),
        out_specs=full((4, 4, 192, 128)),
    )(place, incoming, *[w for w in quad for _ in range(2)])
    hidden_all = exchange(hidden, "g")

    partial = call(
        flash_kernel,
        shape((4, rows_a, 384), BF),
        scratch=[pltpu.VMEM((2, 4, rows_a, 256), F32)],
        count=2,
    )(where, q_all, kv_all)
    partial_all = exchange(partial, "x")

    result = pl.pallas_call(
        down_kernel,
        grid=(1,),
        out_shape=shape((32, 4, 8, 128), BF),
        in_specs=[pl.BlockSpec(memory_space=pltpu.SMEM), full((4, 4, 192, 128))] + weight_specs((2,)),
        out_specs=full((32, 4, 8, 128)),
    )(place, hidden_all, *quad)
    returned = exchange(result.reshape(128, 8, 128), EP + QUAD)

    head_send = call(mix_kernel, shape((16, rows_a // 2, 128), BF), count=2)(
        mix_lambda, partial_all, head_gain[None]
    )
    head_all = exchange(head_send, TP)
    mine, theirs = call(
        project_kernel,
        (shape((rows_a // 2, 128), BF), shape((rows_a // 2, 128), BF)),
        smem_first=False,
        count=3,
    )(head_all, w_mix_out, other_out)
    received = swap(theirs, "c", 2, 1)
    attn_out = jnp.where(
        core == 0,
        jnp.concatenate([mine, received], axis=0),
        jnp.concatenate([received, mine], axis=0),
    )

    moe_out = call(combine_kernel, shape((rows_b, 128), BF), smem_first=False, count=3)(
        routes_t, route_weight.T, returned
    )
    return (attn_out, moe_out)


def solution(mesh):
    finer = Mesh(mesh.devices.reshape(8, 4, 4, 2, 2), ("z", "x", "g", "r", "c"))
    placed = (
        P(EP, None),
        P(),
        P(None, TP),
        P(None, TP),
        P(None, TP),
        P(),
        P(),
        P(TP),
        P(),
        P(None, TP),
        P(EP, None),
        P(),
        P(EP, None),
        P(EP, None),
        P(EP, None, TP),
        P(EP, None, TP),
        P(EP, None, TP),
    )
    return jax.shard_map(
        body, mesh=finer, in_specs=placed, out_specs=(P(EP, TP), P(EP, TP)), check_vma=False
    )
```

time: 242 us -> 171 us (0.71); the launches traced: 238 us -> 170 us
  blocking collectives: 102 us -> 10.6 us
  starting transfers between devices: 9.28 us -> 53.7 us
  Pallas kernels: 0 us -> 28 us
  matrix products: 26.8 us -> 0 us
  between operations: 14.8 us -> 1.54 us
  local copies, waits for them, and re-layouts: 13.3 us -> 1.71 us
  waiting for transfers between devices: 62.3 us -> 70.6 us
  other arithmetic: 8.72 us -> 3.45 us
    all_to_all x1, blocking collectives: 97.3 us -> 10.6 us  [exchange(): return lax.all_to_all(a, axes, 0, 0, tiled=True)]
    all_to_all x1 -> x6, waiting for transfers between devices: 0.01 us -> 69.6 us  [exchange(): return lax.all_to_all(a, axes, 0, 0, tiled=True)]
    all_gather x3 -> x0, waiting for transfers between devices: 62.3 us -> none  [the longest x1 28.2 us: route_experts(): lax.all_gather(hidden, TP, axis=1, tiled=True)]
    all_to_all x1 -> x6, starting transfers between devices: 8.98 us -> 38.6 us  [exchange(): return lax.all_to_all(a, axes, 0, 0, tiled=True)]
    pallas_call x0 -> x8, Pallas kernels: none -> 28 us  [the longest x1 5.71 us: body(): pl.pallas_call(hidden_kernel, grid=(1,), out_shape=shape((4, 4, 192, 128)...]
    dot_general x9 -> x0, matrix products: 26.8 us -> none  [the longest x1 7.57 us: attend(): jnp.einsum('qhcd,khcd->cqhk', queries, key_piece, preferred_element_type=...]
    ppermute x0 -> x5, starting transfers between devices: none -> 15 us  [swap(): return lax.ppermute(a, axes, [(n, n ^ flip) for n in range(size)])]
    gather x2 -> x0, local copies, waits for them, and re-layouts: 5.6 us -> none  [the longest x1 4.27 us: route_experts(): normed[source]]
  transfers between devices with their start and end apart: 4 -> 11, of which waited for: 3 -> 7; matrix products, arithmetic and copies ran while one was open for 17% -> 1% of each run, Pallas kernels for 0% -> 13%
where the time goes in v1:
time: 171 us; the launch traced here: 170 us
  waiting for transfers between devices  70.6 us (41%)
  starting transfers between devices  53.7 us (31%)
  Pallas kernels  28 us (16%)
  blocking collectives  10.6 us (6%)
  other arithmetic  3.45 us (2%)
  local copies, waits for them, and re-layouts  1.71 us (1%)
    all_to_all x6, waiting for transfers between devices, exchange(): return lax.all_to_all(a, axes, 0, 0, tiled=True)  69.6 us
    all_to_all x6, starting transfers between devices, exchange(): return lax.all_to_all(a, axes, 0, 0, tiled=True)  38.6 us
    ppermute x5, starting transfers between devices, swap(): return lax.ppermute(a, axes, [(n, n ^ flip) for n in range(size)])  15 us
    all_to_all x1, blocking collectives, exchange(): return lax.all_to_all(a, axes, 0, 0, tiled=True)  10.6 us
    pallas_call x1, Pallas kernels, body(): pl.pallas_call(hidden_kernel, grid=(1,), out_shape=shape((4, 4, 192, 128)...  5.71 us
    pallas_call x1, Pallas kernels, body(): pl.pallas_call(down_kernel, grid=(1,), out_shape=shape((32, 4, 8, 128), B...  4.16 us
    pallas_call x1, Pallas kernels, body(): call(qkv_kernel, (shape((4, rows_a, 128), BF), shape((8, rows_a, 256), BF...  3.95 us
    pallas_call x1, Pallas kernels, body(): call(flash_kernel, shape((4, rows_a, 384), BF), scratch=[pltpu.VMEM((2, 4...  3.79 us
  transfers between devices with their start and end apart: 11, of which 7 were waited for; matrix products, arithmetic and copies ran while one was open for 1% of the time, Pallas kernels for 13%

profile of v1, /device:TPU:1, one launch (start us, length us, event | category | flops | bytes accessed | tf_op | source)
XLA Modules:
  0.0 169.6 jit_solution(6335158879185032999)
XLA Ops:
  0.6 1.3 maximum_bitcast_fusion
  2.0 4.0 %shard_map.176 = (bf16[4,256,128]{2,1,0:T(8,128)(2,1)}, bf16[8,256,256]{2,1,0:T(8,128)(2,1)}) custom-call(bf16[256,2048]{1,0:T(8,128)(2,1)} %x_ref.2, f32[1,2048]{1,0:T(1,128)} %bitcast.14, bf16[2048,128]{1,0:T(8,128)(2,1)} %wq_ref.1, bf16[2048,128]{1,0:T(8,128)(2,1)} %wk_ref.1, bf16[2048,128]{1,0:T(8,128)(2,1)} %wv_ref.1, ...), custom_call_target="tpu_custom_call" | custom-call | tf_op jit(solution)/shard_map/pallas_call | solution.py:281
  5.9 10.6 %all_to_all.35.q_ref = bf16[4,256,128]{2,1,0:T(8,128)(2,1)} all-to-all(bf16[4,256,128]{2,1,0:T(8,128)(2,1)} %get-tuple-element.6), channel_id=1, replica_groups=mesh['z'=8,'x'=4,'g'=4,'r'=2,'c'=2] {'x'}, dimensions={0} | all-to-all | bytes 524288 | tf_op jit(solution)/shard_map/all_to_all | solution.py:234
  16.5 10.2 %all-to-all-start.1 = ((bf16[8,256,256]{2,1,0:T(8,128)(2,1)}), bf16[8,256,256]{2,1,0:T(8,128)(2,1)}, u32[]{:S(2)}, u32[]{:S(2)}) async-start(bf16[8,256,256]{2,1,0:T(8,128)(2,1)} %get-tuple-element.7), calls=%async_computation.1 | async-start | bytes 2097152 | tf_op jit(solution)/shard_map/all_to_all | solution.py:234
  26.9 3.2 %collective-permute-start.3 = (bf16[3,2048,128]{2,1,0:T(8,128)(2,1)S(1)}, bf16[3,2048,128]{2,1,0:T(8,128)(2,1)S(1)}, u32[]{:S(2)}, u32[]{:S(2)}) collective-permute-start(bf16[3,2048,128]{2,1,0:T(8,128)(2,1)S(1)} %constant_dynamic-update-slice_fusion.refs_0_.refs_1_), channel_id=1, source_target_pairs={{0,2},{2,0},{1,3},{3,1},{4,6},{6,4},{5,7},{7,5},{8,10},{10,8},{9,1... | collective-permute-start | bytes 4718600 | tf_op jit(solution)/shard_map/ppermute | solution.py:238
  30.2 3.6 %shard_map.180 = bf16[32,24,512]{2,1,0:T(8,128)(2,1)} custom-call(s32[1]{0:T(128)} %bitcast.8.place_ref, bf16[128,2048]{1,0:T(8,128)(2,1)} %x_ref.3, f32[1,2048]{1,0:T(1,128)} %bitcast.15, s32[4,128]{1,0:T(4,128)} %bitcast.16), custom_call_target="tpu_custom_call" | custom-call | tf_op jit(solution)/shard_map/pallas_call | solution.py:275
  33.8 22.1 %all-to-all-done.1.kv_ref = bf16[8,256,256]{2,1,0:T(8,128)(2,1)} async-done(((bf16[8,256,256]{2,1,0:T(8,128)(2,1)}), bf16[8,256,256]{2,1,0:T(8,128)(2,1)}, u32[]{:S(2)}, u32[]{:S(2)}) %all-to-all-start.1) | async-done | bytes 1048608 | tf_op jit(solution)/shard_map/all_to_all | solution.py:234
  55.9 4.6 %all-to-all-start.4 = ((bf16[32,24,512]{2,1,0:T(8,128)(2,1)}), bf16[32,24,512]{2,1,0:T(8,128)(2,1)}, u32[]{:S(2)}, u32[]{:S(2)}) async-start(bf16[32,24,512]{2,1,0:T(8,128)(2,1)} %shard_map.180), calls=%async_computation.4 | async-start | bytes 1572864 | tf_op jit(solution)/shard_map/all_to_all | solution.py:234
  60.5 2.5 %collective-permute-start.2 = (bf16[3,2048,128]{2,1,0:T(8,128)(2,1)S(1)}, bf16[3,2048,128]{2,1,0:T(8,128)(2,1)}, u32[]{:S(2)}, u32[]{:S(2)}) collective-permute-start(bf16[3,2048,128]{2,1,0:T(8,128)(2,1)S(1)} %constant_dynamic-update-slice_fusion.refs_0_.refs_1_), channel_id=1, source_target_pairs={{0,1},{1,0},{2,3},{3,2},{4,5},{5,4},{6,7},{7,6},{8,9},{9,8},{10,11... | collective-permute-start | bytes 4718600 | tf_op jit(solution)/shard_map/ppermute | solution.py:238
  63.1 4.5 %collective-permute-start.4 = (bf16[3,2048,128]{2,1,0:T(8,128)(2,1)S(1)}, bf16[3,2048,128]{2,1,0:T(8,128)(2,1)}, u32[]{:S(2)}, u32[]{:S(2)}) collective-permute-start(bf16[3,2048,128]{2,1,0:T(8,128)(2,1)S(1)} %collective-permute-done.3.refs_4_.refs_5_.refs_2_), channel_id=1, source_target_pairs={{0,1},{1,0},{2,3},{3,2},{4,5},{5,4},{6,7},{7,6},{8,9},{9,8},{10,11... | collective-permute-start | bytes 4718600 | tf_op jit(solution)/shard_map/ppermute | solution.py:238
  67.6 0.7 pad_add_fusion.place_ref
  68.2 3.8 %shard_map.177 = bf16[4,256,384]{2,1,0:T(8,128)(2,1)} custom-call(s32[2]{0:T(128)} %pad_add_fusion.place_ref, bf16[4,256,128]{2,1,0:T(8,128)(2,1)} %all_to_all.35.q_ref, bf16[8,256,256]{2,1,0:T(8,128)(2,1)} %all-to-all-done.1.kv_ref), custom_call_target="tpu_custom_call" | custom-call | tf_op jit(solution)/shard_map/pallas_call | solution.py:303
  72.0 9.8 %all-to-all-done.4.in_ref = bf16[32,24,512]{2,1,0:T(8,128)(2,1)} async-done(((bf16[32,24,512]{2,1,0:T(8,128)(2,1)}), bf16[32,24,512]{2,1,0:T(8,128)(2,1)}, u32[]{:S(2)}, u32[]{:S(2)}) %all-to-all-start.4) | async-done | bytes 786464 | tf_op jit(solution)/shard_map/all_to_all | solution.py:234
  81.8 4.6 %all-to-all-start.2 = ((bf16[4,256,384]{2,1,0:T(8,128)(2,1)}), bf16[4,256,384]{2,1,0:T(8,128)(2,1)}, u32[]{:S(2)}, u32[]{:S(2)}) async-start(bf16[4,256,384]{2,1,0:T(8,128)(2,1)} %shard_map.177), calls=%async_computation.2 | async-start | bytes 1572864 | tf_op jit(solution)/shard_map/all_to_all | solution.py:234
  86.3 5.7 %shard_map.181 = bf16[4,4,192,128]{3,2,1,0:T(8,128)(2,1)} custom-call(s32[1]{0:T(128)} %bitcast.8.place_ref, bf16[32,24,512]{2,1,0:T(8,128)(2,1)} %all-to-all-done.4.in_ref, bf16[3,2048,128]{2,1,0:T(8,128)(2,1)} %copy-done, bf16[3,2048,128]{2,1,0:T(8,128)(2,1)} %copy-done, bf16[3,2048,128]{2,1,0:T(8,128)(2,1)} %collective-permute-done.2.refs_2_.refs_3_.refs_1_, ...), custom_call_target="tpu_custom_call" | custom-call | tf_op jit(solution)/shard_map/pallas_call | solution.py:294
  92.1 4.1 %all-to-all-done.2.part_ref = bf16[4,256,384]{2,1,0:T(8,128)(2,1)} async-done(((bf16[4,256,384]{2,1,0:T(8,128)(2,1)}), bf16[4,256,384]{2,1,0:T(8,128)(2,1)}, u32[]{:S(2)}, u32[]{:S(2)}) %all-to-all-start.2) | async-done | bytes 786464 | tf_op jit(solution)/shard_map/all_to_all | solution.py:234
  96.2 6.8 %all-to-all-start.5 = ((bf16[4,4,192,128]{3,2,1,0:T(8,128)(2,1)}), bf16[4,4,192,128]{3,2,1,0:T(8,128)(2,1)S(1)}, u32[]{:S(2)}, u32[]{:S(2)}) async-start(bf16[4,4,192,128]{3,2,1,0:T(8,128)(2,1)} %shard_map.181), calls=%async_computation.5 | async-start | bytes 1572864 | tf_op jit(solution)/shard_map/all_to_all | solution.py:234
  103.8 2.2 %shard_map.178 = bf16[16,128,128]{2,1,0:T(8,128)(2,1)} custom-call(f32[1]{0:T(128)S(6)} %copy.21.lam_ref, bf16[4,256,384]{2,1,0:T(8,128)(2,1)} %all-to-all-done.2.part_ref, f32[1,128]{1,0:T(1,128)} %bitcast.19), custom_call_target="tpu_custom_call" | custom-call | tf_op jit(solution)/shard_map/pallas_call | solution.py:320
  106.0 17.5 %all-to-all-done.5.hidden_ref = bf16[4,4,192,128]{3,2,1,0:T(8,128)(2,1)S(1)} async-done(((bf16[4,4,192,128]{3,2,1,0:T(8,128)(2,1)}), bf16[4,4,192,128]{3,2,1,0:T(8,128)(2,1)S(1)}, u32[]{:S(2)}, u32[]{:S(2)}) %all-to-all-start.5) | async-done | bytes 786464 | tf_op jit(solution)/shard_map/all_to_all | solution.py:234
  123.5 5.5 %all-to-all-start.3 = ((bf16[16,128,128]{2,1,0:T(8,128)(2,1)}), bf16[16,128,128]{2,1,0:T(8,128)(2,1)S(1)}, u32[]{:S(2)}, u32[]{:S(2)}) async-start(bf16[16,128,128]{2,1,0:T(8,128)(2,1)} %shard_map.178), calls=%async_computation.3 | async-start | bytes 1048576 | tf_op jit(solution)/shard_map/all_to_all | solution.py:234
  129.0 2.0 %collective-permute-start = (bf16[2048,128]{1,0:T(8,128)(2,1)S(1)}, bf16[2048,128]{1,0:T(8,128)(2,1)S(1)}, u32[]{:S(2)}, u32[]{:S(2)}) collective-permute-start(bf16[2048,128]{1,0:T(8,128)(2,1)S(1)} %copy-done.5), channel_id=1, source_target_pairs={{0,1},{1,0},{2,3},{3,2},{4,5},{5,4},{6,7},{7,6},{8,9},{9,8},{10,11... | collective-permute-start | bytes 1572872 | tf_op jit(solution)/shard_map/ppermute | solution.py:238
  131.0 4.2 %shard_map.182 = bf16[32,4,8,128]{3,2,1,0:T(8,128)(2,1)} custom-call(s32[1]{0:T(128)} %bitcast.8.place_ref, bf16[4,4,192,128]{3,2,1,0:T(8,128)(2,1)} %copy-done.2, bf16[3,2048,128]{2,1,0:T(8,128)(2,1)} %copy-done, bf16[3,2048,128]{2,1,0:T(8,128)(2,1)} %collective-permute-done.2.refs_2_.refs_3_.refs_1_, bf16[3,2048,128]{2,1,0:T(8,128)(2,1)} %copy-done.1, ...), custom_call_target="tpu_custom_call" | custom-call | tf_op jit(solution)/shard_map/pallas_call | solution.py:311
  135.2 11.0 %all-to-all-done.3.rows_ref = bf16[16,128,128]{2,1,0:T(8,128)(2,1)S(1)} async-done(((bf16[16,128,128]{2,1,0:T(8,128)(2,1)}), bf16[16,128,128]{2,1,0:T(8,128)(2,1)S(1)}, u32[]{:S(2)}, u32[]{:S(2)}) %all-to-all-start.3) | async-done | bytes 524320 | tf_op jit(solution)/shard_map/all_to_all | solution.py:234
  146.2 6.9 %all-to-all-start.6 = ((bf16[128,8,128]{2,1,0:T(8,128)(2,1)}), bf16[128,8,128]{2,1,0:T(8,128)(2,1)S(1)}, u32[]{:S(2)}, u32[]{:S(2)}) async-start(bf16[128,8,128]{2,1,0:T(8,128)(2,1)} %bitcast.13), calls=%async_computation.6 | async-start | bytes 524288 | tf_op jit(solution)/shard_map/all_to_all | solution.py:234
  153.1 0.8 copy-done.6
  153.9 2.4 %shard_map.179 = (bf16[128,128]{1,0:T(8,128)(2,1)}, bf16[128,128]{1,0:T(8,128)(2,1)}) custom-call(bf16[16,128,128]{2,1,0:T(8,128)(2,1)} %copy-done.3, bf16[2048,128]{1,0:T(8,128)(2,1)} %own_ref.1, bf16[2048,128]{1,0:T(8,128)(2,1)} %copy-done.6), custom_call_target="tpu_custom_call" | custom-call | tf_op jit(solution)/shard_map/pallas_call | solution.py:324
  156.3 2.8 %collective-permute-start.1 = (bf16[128,128]{1,0:T(8,128)(2,1)}, bf16[128,128]{1,0:T(8,128)(2,1)S(1)}, u32[]{:S(2)}, u32[]{:S(2)}) collective-permute-start(bf16[128,128]{1,0:T(8,128)(2,1)} %get-tuple-element.9), channel_id=1, source_target_pairs={{0,1},{1,0},{2,3},{3,2},{4,5},{5,4},{6,7},{7,6},{8,9},{9,8},{10,11... | collective-permute-start | bytes 98312 | tf_op jit(solution)/shard_map/ppermute | solution.py:238
  159.1 1.0 collective-permute-done.1
  160.2 1.5 maximum_select_fusion
  161.6 5.1 %all-to-all-done.6.rows_ref = bf16[128,8,128]{2,1,0:T(8,128)(2,1)S(1)} async-done(((bf16[128,8,128]{2,1,0:T(8,128)(2,1)}), bf16[128,8,128]{2,1,0:T(8,128)(2,1)S(1)}, u32[]{:S(2)}, u32[]{:S(2)}) %all-to-all-start.6) | async-done | bytes 262176 | tf_op jit(solution)/shard_map/all_to_all | solution.py:234
  166.7 0.7 copy-done.4
  167.4 2.2 %shard_map.183 = bf16[128,128]{1,0:T(8,128)(2,1)} custom-call(s32[4,128]{1,0:T(4,128)} %bitcast.17, f32[4,128]{1,0:T(4,128)} %bitcast.18, bf16[128,8,128]{2,1,0:T(8,128)(2,1)} %copy-done.4), custom_call_target="tpu_custom_call" | custom-call | tf_op jit(solution)/shard_map/pallas_call | solution.py:337
  (25 shorter events, 0.2 us)
Async XLA Ops:
  5.9 20.8 %copy-start.7 = (bf16[1,2048,128]{2,1,0:T(8,128)(2,1)S(1)}, bf16[1,2048,128]{2,1,0:T(8,128)(2,1)}, u32[]{:S(2)}) copy-start(bf16[1,2048,128]{2,1,0:T(8,128)(2,1)} %param.31) | copy-start | bytes 1572868
  16.5 10.3 %copy-start.8 = (bf16[1,2048,128]{2,1,0:T(8,128)(2,1)S(1)}, bf16[1,2048,128]{2,1,0:T(8,128)(2,1)}, u32[]{:S(2)}) copy-start(bf16[1,2048,128]{2,1,0:T(8,128)(2,1)} %param.32) | copy-start | bytes 1572868
  16.5 10.3 %copy-start.9 = (bf16[1,2048,128]{2,1,0:T(8,128)(2,1)S(1)}, bf16[1,2048,128]{2,1,0:T(8,128)(2,1)}, u32[]{:S(2)}) copy-start(bf16[1,2048,128]{2,1,0:T(8,128)(2,1)} %param.33) | copy-start | bytes 1572868
  16.5 39.4 %all-to-all-start.1 = ((bf16[8,256,256]{2,1,0:T(8,128)(2,1)}), bf16[8,256,256]{2,1,0:T(8,128)(2,1)}, u32[]{:S(2)}, u32[]{:S(2)}) async-start(bf16[8,256,256]{2,1,0:T(8,128)(2,1)} %get-tuple-element.7), calls=%async_computation.1 | async-start | bytes 2097152 | tf_op jit(solution)/shard_map/all_to_all | solution.py:234
  26.9 45.1 %copy-start = (bf16[3,2048,128]{2,1,0:T(8,128)(2,1)}, bf16[3,2048,128]{2,1,0:T(8,128)(2,1)S(1)}, u32[]{:S(2)}) copy-start(bf16[3,2048,128]{2,1,0:T(8,128)(2,1)S(1)} %constant_dynamic-update-slice_fusion.refs_0_.refs_1_) | copy-start | bytes 4718596
  26.9 36.1 %collective-permute-start.3 = (bf16[3,2048,128]{2,1,0:T(8,128)(2,1)S(1)}, bf16[3,2048,128]{2,1,0:T(8,128)(2,1)S(1)}, u32[]{:S(2)}, u32[]{:S(2)}) collective-permute-start(bf16[3,2048,128]{2,1,0:T(8,128)(2,1)S(1)} %constant_dynamic-update-slice_fusion.refs_0_.refs_1_), channel_id=1, source_target_pairs={{0,2},{2,0},{1,3},{3,1},{4,6},{6,4},{5,7},{7,5},{8,10},{10,8},{9,1... | collective-permute-start | bytes 4718600 | tf_op jit(solution)/shard_map/ppermute | solution.py:238
  55.9 25.9 %all-to-all-start.4 = ((bf16[32,24,512]{2,1,0:T(8,128)(2,1)}), bf16[32,24,512]{2,1,0:T(8,128)(2,1)}, u32[]{:S(2)}, u32[]{:S(2)}) async-start(bf16[32,24,512]{2,1,0:T(8,128)(2,1)} %shard_map.180), calls=%async_computation.4 | async-start | bytes 1572864 | tf_op jit(solution)/shard_map/all_to_all | solution.py:234
  60.5 25.8 %collective-permute-start.2 = (bf16[3,2048,128]{2,1,0:T(8,128)(2,1)S(1)}, bf16[3,2048,128]{2,1,0:T(8,128)(2,1)}, u32[]{:S(2)}, u32[]{:S(2)}) collective-permute-start(bf16[3,2048,128]{2,1,0:T(8,128)(2,1)S(1)} %constant_dynamic-update-slice_fusion.refs_0_.refs_1_), channel_id=1, source_target_pairs={{0,1},{1,0},{2,3},{3,2},{4,5},{5,4},{6,7},{7,6},{8,9},{9,8},{10,11... | collective-permute-start | bytes 4718600 | tf_op jit(solution)/shard_map/ppermute | solution.py:238
  63.1 18.7 %copy-start.1 = (bf16[3,2048,128]{2,1,0:T(8,128)(2,1)}, bf16[3,2048,128]{2,1,0:T(8,128)(2,1)S(1)}, u32[]{:S(2)}) copy-start(bf16[3,2048,128]{2,1,0:T(8,128)(2,1)S(1)} %collective-permute-done.3.refs_4_.refs_5_.refs_2_) | copy-start | bytes 4718596
  63.1 23.3 %collective-permute-start.4 = (bf16[3,2048,128]{2,1,0:T(8,128)(2,1)S(1)}, bf16[3,2048,128]{2,1,0:T(8,128)(2,1)}, u32[]{:S(2)}, u32[]{:S(2)}) collective-permute-start(bf16[3,2048,128]{2,1,0:T(8,128)(2,1)S(1)} %collective-permute-done.3.refs_4_.refs_5_.refs_2_), channel_id=1, source_target_pairs={{0,1},{1,0},{2,3},{3,2},{4,5},{5,4},{6,7},{7,6},{8,9},{9,8},{10,11... | collective-permute-start | bytes 4718600 | tf_op jit(solution)/shard_map/ppermute | solution.py:238
  81.8 14.4 %all-to-all-start.2 = ((bf16[4,256,384]{2,1,0:T(8,128)(2,1)}), bf16[4,256,384]{2,1,0:T(8,128)(2,1)}, u32[]{:S(2)}, u32[]{:S(2)}) async-start(bf16[4,256,384]{2,1,0:T(8,128)(2,1)} %shard_map.177), calls=%async_computation.2 | async-start | bytes 1572864 | tf_op jit(solution)/shard_map/all_to_all | solution.py:234
  96.2 27.3 %all-to-all-start.5 = ((bf16[4,4,192,128]{3,2,1,0:T(8,128)(2,1)}), bf16[4,4,192,128]{3,2,1,0:T(8,128)(2,1)S(1)}, u32[]{:S(2)}, u32[]{:S(2)}) async-start(bf16[4,4,192,128]{3,2,1,0:T(8,128)(2,1)} %shard_map.181), calls=%async_computation.5 | async-start | bytes 1572864 | tf_op jit(solution)/shard_map/all_to_all | solution.py:234
  103.0 26.0 %copy-start.5 = (bf16[2048,128]{1,0:T(8,128)(2,1)S(1)}, bf16[2048,128]{1,0:T(8,128)(2,1)}, u32[]{:S(2)}) copy-start(bf16[2048,128]{1,0:T(8,128)(2,1)} %own_ref.1) | copy-start | bytes 1572868
  123.5 7.6 %copy-start.2 = (bf16[4,4,192,128]{3,2,1,0:T(8,128)(2,1)}, bf16[4,4,192,128]{3,2,1,0:T(8,128)(2,1)S(1)}, u32[]{:S(2)}) copy-start(bf16[4,4,192,128]{3,2,1,0:T(8,128)(2,1)S(1)} %all-to-all-done.5.hidden_ref) | copy-start | bytes 2359300
  123.5 22.8 %all-to-all-start.3 = ((bf16[16,128,128]{2,1,0:T(8,128)(2,1)}), bf16[16,128,128]{2,1,0:T(8,128)(2,1)S(1)}, u32[]{:S(2)}, u32[]{:S(2)}) async-start(bf16[16,128,128]{2,1,0:T(8,128)(2,1)} %shard_map.178), calls=%async_computation.3 | async-start | bytes 1048576 | tf_op jit(solution)/shard_map/all_to_all | solution.py:234
  129.0 24.1 %collective-permute-start = (bf16[2048,128]{1,0:T(8,128)(2,1)S(1)}, bf16[2048,128]{1,0:T(8,128)(2,1)S(1)}, u32[]{:S(2)}, u32[]{:S(2)}) collective-permute-start(bf16[2048,128]{1,0:T(8,128)(2,1)S(1)} %copy-done.5), channel_id=1, source_target_pairs={{0,1},{1,0},{2,3},{3,2},{4,5},{5,4},{6,7},{7,6},{8,9},{9,8},{10,11... | collective-permute-start | bytes 1572872 | tf_op jit(solution)/shard_map/ppermute | solution.py:238
  146.2 6.9 %copy-start.3 = (bf16[16,128,128]{2,1,0:T(8,128)(2,1)}, bf16[16,128,128]{2,1,0:T(8,128)(2,1)S(1)}, u32[]{:S(2)}) copy-start(bf16[16,128,128]{2,1,0:T(8,128)(2,1)S(1)} %all-to-all-done.3.rows_ref) | copy-start | bytes 1572868
  146.2 20.5 %all-to-all-start.6 = ((bf16[128,8,128]{2,1,0:T(8,128)(2,1)}), bf16[128,8,128]{2,1,0:T(8,128)(2,1)S(1)}, u32[]{:S(2)}, u32[]{:S(2)}) async-start(bf16[128,8,128]{2,1,0:T(8,128)(2,1)} %bitcast.13), calls=%async_computation.6 | async-start | bytes 524288 | tf_op jit(solution)/shard_map/all_to_all | solution.py:234
  153.1 0.8 copy-start.6
  156.3 3.8 %collective-permute-start.1 = (bf16[128,128]{1,0:T(8,128)(2,1)}, bf16[128,128]{1,0:T(8,128)(2,1)S(1)}, u32[]{:S(2)}, u32[]{:S(2)}) collective-permute-start(bf16[128,128]{1,0:T(8,128)(2,1)} %get-tuple-element.9), channel_id=1, source_target_pairs={{0,1},{1,0},{2,3},{3,2},{4,5},{5,4},{6,7},{7,6},{8,9},{9,8},{10,11... | collective-permute-start | bytes 98312 | tf_op jit(solution)/shard_map/ppermute | solution.py:238
  166.7 0.7 copy-start.4

commit v2 on v1

v2 whole, which is shorter than its diff:
```python
import jax
import jax.numpy as jnp
from jax import lax
from jax.experimental import pallas as pl
from jax.experimental.pallas import tpu as pltpu
from jax.sharding import Mesh
from jax.sharding import PartitionSpec as P


BF = jnp.bfloat16
F32 = jnp.float32
EP = ("w", "v", "x")
TP = ("g", "r", "c")
QUAD = ("r", "c")


def dot(a, b, dims=((1,), (0,))):
    return lax.dot_general(a, b, (dims, ((), ())), preferred_element_type=F32)


def call(kernel, shapes, scratch=(), smem_first=True, count=0):
    specs = [pl.BlockSpec(memory_space=pltpu.VMEM)] * count
    if smem_first:
        specs = [pl.BlockSpec(memory_space=pltpu.SMEM)] + specs
    multiple = isinstance(shapes, (list, tuple))
    out_specs = pl.BlockSpec(memory_space=pltpu.VMEM)
    return pl.pallas_call(
        kernel,
        out_shape=tuple(shapes) if multiple else shapes,
        in_specs=specs,
        out_specs=tuple([out_specs] * len(shapes)) if multiple else out_specs,
        scratch_shapes=list(scratch),
    )


def corner():
    return lax.axis_index("r") * 2 + lax.axis_index("c")


def rms(wide, gain, epsilon):
    scale = lax.rsqrt(jnp.mean(wide * wide, axis=-1, keepdims=True) + epsilon)
    return wide * scale * gain


def expert_tables(routes_ref, experts):
    tokens = routes_ref.shape[1]
    expert = lax.broadcasted_iota(jnp.int32, (experts, tokens), 0)
    named = jnp.zeros((experts, tokens), jnp.bool_)
    for k in range(routes_ref.shape[0]):
        named = named | (routes_ref[k : k + 1, :] == expert)
    earlier = lax.broadcasted_iota(jnp.int32, (tokens, tokens), 0) < lax.broadcasted_iota(
        jnp.int32, (tokens, tokens), 1
    )
    counts = dot(
        jnp.where(named, 1.0, 0.0).astype(BF), jnp.where(earlier, 1.0, 0.0).astype(BF)
    )
    return jnp.where(named, counts, -1.0), expert


def spread(table, times):
    rows, lanes = table.shape
    return jnp.broadcast_to(table[:, None, :], (rows, times, lanes)).reshape(rows * times, lanes)


def dispatch_kernel(x_ref, gain_ref, routes_ref, out_ref):
    experts = out_ref.shape[0]
    position, _ = expert_tables(routes_ref, experts)
    _, width = x_ref.shape
    chunk = width // 4
    wide = spread(position, 24)
    row = lax.broadcasted_iota(jnp.int32, wide.shape, 0) % 24
    wanted = (row % 6 + 6 * corner()).astype(F32)
    hit = wide == wanted
    normed = rms(x_ref[...].astype(F32), gain_ref[...], 1e-05).astype(BF)
    total = None
    for part in range(4):
        pick = jnp.where(hit & (row // 6 == part), 1.0, 0.0).astype(BF)
        piece = dot(pick, normed[:, part * chunk : (part + 1) * chunk])
        total = piece if total is None else total + piece
    out_ref[...] = total.astype(BF).reshape(out_ref.shape)


def qkv_kernel(x_ref, gain_ref, wq_ref, wk_ref, wv_ref, qg_ref, kg_ref, q_ref, kv_ref):
    normed = rms(x_ref[...].astype(F32), gain_ref[...], 1e-05).astype(BF)

    def component_norm(wide, gain):
        low = lax.broadcasted_iota(jnp.int32, wide.shape, 1) < 64
        square = wide * wide
        first = jnp.sum(jnp.where(low, square, 0.0), axis=-1, keepdims=True)
        second = jnp.sum(jnp.where(low, 0.0, square), axis=-1, keepdims=True)
        scale = jnp.where(
            low, lax.rsqrt(first / 64 + 1e-06), lax.rsqrt(second / 64 + 1e-06)
        )
        return wide * scale * jnp.concatenate([gain, gain], axis=1)

    q = (component_norm(dot(normed, wq_ref[...]), qg_ref[...]) * 0.125).astype(BF)
    k = component_norm(dot(normed, wk_ref[...]), kg_ref[...]).astype(BF)
    v = dot(normed, wv_ref[...]).astype(BF)
    q_ref[...] = q
    kv_ref[:, 0:128] = k
    kv_ref[:, 128:256] = v


def flash_kernel(*refs):
    q_refs, kv_refs, outs, total_ref, q_all = refs[0:4], refs[4:8], refs[8:12], refs[12], refs[13]
    w, v, x = (lax.axis_index(name) for name in EP)
    rows = q_refs[0].shape[0]
    keys = kv_refs[0].shape[0]
    half = keys // 2
    ones = jnp.ones((keys, 128), BF)
    for n in range(4):
        q_all[n] = q_refs[n][...]

    def attend(n, masked):
        for comp in range(2):
            lanes = slice(64 * comp, 64 * comp + 64)
            q = q_all[n, :, lanes]
            total = None
            for turn in range(4):
                kv = kv_refs[turn][...]
                value = jnp.concatenate([kv[:, 128:256], ones], axis=1)
                weight = jnp.exp(dot(q, kv[:, lanes], ((1,), (1,))))
                if masked:
                    source = (x + turn) % 4
                    first = 1024 * v + 256 * source
                    second = 1024 * (1 - v) + 256 * source
                    mine = 1024 * v + 256 * x
                    col = lax.broadcasted_iota(jnp.int32, weight.shape, 1)
                    row = lax.broadcasted_iota(jnp.int32, weight.shape, 0)
                    key_pos = jnp.where(col < half, col + first, col - half + second)
                    weight = jnp.where(key_pos <= row + mine, weight, 0.0)
                piece = dot(weight.astype(BF), value)
                total = piece if total is None else total + piece
            total_ref[n, comp] = total

    attend(0, True)

    def later(n, carry):
        attend(n, False)
        return carry

    lax.fori_loop(1, 4 - w, later, 0)
    for n in range(4):

        @pl.when(n + w < 4)
        def _():
            lines = []
            for comp in range(2):
                outs[n][0:rows, 128 * comp : 128 * comp + 128] = total_ref[n, comp, :, 0:128].astype(BF)
                sums = total_ref[n, comp, :, 128:256].T[0:1]
                high = sums.astype(BF).astype(F32)
                lines += [high, sums - high]
            outs[n][rows:, :] = jnp.concatenate(lines + [jnp.zeros((4, rows), F32)], axis=0).astype(BF)


def mix_kernel(lam_ref, *refs):
    parts, gain_ref, out_ref = refs[0:4], refs[4], refs[5]
    total = parts[0][...].astype(F32)
    for n in range(1, 4):
        total = total + parts[n][...].astype(F32)
    rows = total.shape[1]
    lines = total[rows:, :]
    lines = jnp.concatenate([lines, jnp.zeros((120, rows), F32)], axis=0).T
    first = lines[:, 0:1] + lines[:, 1:2]
    second = lines[:, 2:3] + lines[:, 3:4]
    mix = total[0:rows, 0:128] / first - lam_ref[0] * total[0:rows, 128:256] / second
    rows = (rms(mix, gain_ref[...], 1e-05) * 0.8).astype(BF)
    half = rows.shape[0] // 2
    for n in range(out_ref.shape[0] // 2):
        out_ref[2 * n] = rows[0:half]
        out_ref[2 * n + 1] = rows[half:]


def project_kernel(rows_ref, own_ref, other_ref, out_ref, other_out):
    rows = jnp.concatenate([rows_ref[n] for n in range(rows_ref.shape[0])], axis=1)
    count = rows.shape[0]
    spot = pl.multiple_of(lax.axis_index("c") * count, count)
    out_ref[pl.ds(spot, count), :] = dot(rows, own_ref[...]).astype(BF)
    other_out[...] = dot(rows, other_ref[...]).astype(BF)


def finish_kernel(out_ref, received_ref, done_ref):
    count = received_ref.shape[0]
    core = lax.axis_index("c")
    done_ref[...] = out_ref[...]
    done_ref[pl.ds(pl.multiple_of((1 - core) * count, count), count), :] = received_ref[...]


def hidden_kernel(in_ref, *refs):
    weights, out_ref = refs[:-1], refs[-1]
    place = corner()
    sources = in_ref.shape[0]
    flat = in_ref[...].reshape(sources * 24, in_ref.shape[2])
    count = sources * 6
    line = lax.broadcasted_iota(jnp.int32, (count, sources * 24), 0)
    slot = lax.broadcasted_iota(jnp.int32, (count, sources * 24), 1)
    base = (line // 6) * 24 + line % 6
    pieces = []
    for part in range(4):
        pick = jnp.where(slot == base + 6 * part, 1.0, 0.0).astype(BF)
        pieces.append(dot(pick, flat).astype(BF))
    rows = jnp.concatenate(pieces, axis=1)
    for n in range(4):
        gate = jnp.minimum(dot(rows, weights[2 * n][0]), 7.0)
        up = jnp.clip(dot(rows, weights[2 * n + 1][0]), -7.0, 7.0)
        hidden = (gate * jax.nn.sigmoid(1.702 * gate) * (up + 1.0)).astype(BF)
        for peer in range(out_ref.shape[0]):
            out_ref[peer, place ^ n] = hidden


def down_kernel(hidden_ref, *refs):
    weights, out_ref = refs[:-1], refs[-1]
    place = corner()
    rows = jnp.concatenate(
        [hidden_ref[g, a] for g in range(hidden_ref.shape[0]) for a in range(4)], axis=1
    )
    count = rows.shape[0]
    sources = count // 6
    wide = lax.broadcasted_iota(jnp.int32, (sources * 8, count), 0)
    line = lax.broadcasted_iota(jnp.int32, (sources * 8, count), 1)
    hit = ((wide // 8) * 6 + wide % 8 == line) & (wide % 8 < 6)
    pick = jnp.where(hit, 1.0, 0.0).astype(BF)
    for n in range(4):
        result = dot(rows, weights[n][0]).astype(BF)
        result = dot(pick, result).astype(BF)
        out_ref[:, place ^ n] = result.reshape(sources, 8, result.shape[1])


def combine_kernel(routes_ref, weight_ref, rows_ref, out_ref):
    experts = rows_ref.shape[0] // 4
    position, expert = expert_tables(routes_ref, experts)
    weight = jnp.zeros(position.shape, F32)
    for k in range(routes_ref.shape[0]):
        weight = weight + jnp.where(routes_ref[k : k + 1, :] == expert, weight_ref[k : k + 1, :], 0.0)
    wide = spread(position, 32)
    row = lax.broadcasted_iota(jnp.int32, wide.shape, 0) % 32
    slot = jnp.where(row % 8 < 6, (row // 8) * 6 + row % 8, 1000).astype(F32)
    table = jnp.where(wide == slot, spread(weight, 32), 0.0)
    high = table.astype(BF)
    low = (table - high.astype(F32)).astype(BF)
    rows = rows_ref[...].reshape(experts * 32, rows_ref.shape[2])
    dims = ((0,), (0,))
    out_ref[...] = (dot(high, rows, dims) + dot(low, rows, dims)).astype(BF)


def exchange(a, axes):
    return lax.all_to_all(a, axes, 0, 0, tiled=True)


def swap(a, axes, size, flip):
    return lax.ppermute(a, axes, [(n, n ^ flip) for n in range(size)])


def shift(a, axis, size, step, wrap):
    pairs = [(n, (n + step) % size) for n in range(size) if wrap or 0 <= n + step < size]
    return lax.ppermute(a, axis, pairs)


def body(
    x_mix,
    mix_gain,
    w_query,
    w_key,
    w_value,
    query_gain,
    key_gain,
    mix_lambda,
    head_gain,
    w_mix_out,
    x_exp,
    exp_gain,
    routes,
    route_weight,
    w_gate,
    w_up,
    w_down,
):
    shape = jax.ShapeDtypeStruct
    rows_a = x_mix.shape[0]
    rows_b = x_exp.shape[0]

    own = jnp.concatenate([w_gate, w_up, w_down], axis=0)
    far = swap(own, "r", 2, 1)

    routes_t = routes.T
    outgoing = call(dispatch_kernel, shape((32, 24, 512), BF), smem_first=False, count=3)(
        x_exp, exp_gain[None], routes_t
    )
    incoming = exchange(outgoing, EP)

    q_own, kv_own = call(
        qkv_kernel,
        (shape((rows_a, 128), BF), shape((rows_a, 256), BF)),
        smem_first=False,
        count=7,
    )(x_mix, mix_gain[None], w_query, w_key, w_value, query_gain[None], key_gain[None])
    kv_other = swap(kv_own, "v", 2, 1)
    kv_pair = jnp.concatenate([kv_own, kv_other], axis=0)
    kv_all = [kv_pair] + [shift(kv_pair, "x", 4, -n, True) for n in range(1, 4)]
    q_all = [q_own] + [shift(q_own, "w", 4, -n, False) for n in range(1, 4)]

    near = swap(own, "c", 2, 1)
    cross = swap(far, "c", 2, 1)
    other_out = swap(w_mix_out, "c", 2, 1)
    quad = (own, near, far, cross)

    def weight_specs(names):
        return [pl.BlockSpec((1, 2048, 128), lambda n, m=m: (m, 0, 0)) for _ in range(4) for m in names]

    full = lambda s: pl.BlockSpec(s, lambda n: (0,) * len(s))
    hidden = pl.pallas_call(
        hidden_kernel,
        grid=(1,),
        out_shape=shape((4, 4, 192, 128), BF),
        in_specs=[full((32, 24, 512))] + weight_specs((0, 1)),
        out_specs=full((4, 4, 192, 128)),
    )(incoming, *[w for w in quad for _ in range(2)])
    hidden_all = exchange(hidden, "g")

    partial = call(
        flash_kernel,
        [shape((rows_a + 8, 256), BF)] * 4,
        scratch=[pltpu.VMEM((4, 2, rows_a, 256), F32), pltpu.VMEM((4, rows_a, 128), BF)],
        smem_first=False,
        count=8,
    )(*q_all, *kv_all)
    partial_all = [partial[0]] + [shift(partial[n], "w", 4, n, False) for n in range(1, 4)]

    result = pl.pallas_call(
        down_kernel,
        grid=(1,),
        out_shape=shape((32, 4, 8, 128), BF),
        in_specs=[full((4, 4, 192, 128))] + weight_specs((2,)),
        out_specs=full((32, 4, 8, 128)),
    )(hidden_all, *quad)
    returned = exchange(result.reshape(128, 8, 128), EP + QUAD)

    half = rows_a // 2
    head_send = call(mix_kernel, shape((16, half, 128), BF), count=5)(
        mix_lambda, *partial_all, head_gain[None]
    )
    head_all = exchange(head_send, TP)
    mine, theirs = call(
        project_kernel,
        (shape((rows_a, 128), BF), shape((half, 128), BF)),
        smem_first=False,
        count=3,
    )(head_all, w_mix_out, other_out)
    received = swap(theirs, "c", 2, 1)
    attn_out = call(finish_kernel, shape((rows_a, 128), BF), smem_first=False, count=2)(
        mine, received
    )

    moe_out = call(combine_kernel, shape((rows_b, 128), BF), smem_first=False, count=3)(
        routes_t, route_weight.T, returned
    )
    return (attn_out, moe_out)


def solution(mesh):
    finer = Mesh(mesh.devices.reshape(4, 2, 4, 4, 2, 2), EP + TP)
    placed = (
        P(EP, None),
        P(),
        P(None, TP),
        P(None, TP),
        P(None, TP),
        P(),
        P(),
        P(TP),
        P(),
        P(None, TP),
        P(EP, None),
        P(),
        P(EP, None),
        P(EP, None),
        P(EP, None, TP),
        P(EP, None, TP),
        P(EP, None, TP),
    )

    return jax.shard_map(
        body, mesh=finer, in_specs=placed, out_specs=(P(EP, TP), P(EP, TP)), check_vma=False
    )
```

time: 171 us -> 208 us (1.22)
  blocking collectives: 10.6 us -> 35.2 us
  starting transfers between devices: 53.7 us -> 72.5 us
  waiting for transfers between devices: 70.6 us -> 55.5 us
  Pallas kernels: 28 us -> 34 us
  local copies, waits for them, and re-layouts: 1.71 us -> 7.63 us
  other arithmetic: 3.45 us -> 0 us
    all_to_all x6 -> x3, waiting for transfers between devices: 69.6 us -> 15.3 us  [exchange(): return lax.all_to_all(a, axes, 0, 0, tiled=True)]
    ppermute x5 -> x6, waiting for transfers between devices: 1.05 us -> 27 us  [swap(): return lax.ppermute(a, axes, [(n, n ^ flip) for n in range(size)])]
    all_to_all x1, blocking collectives: 10.6 us -> 35.2 us  [exchange(): return lax.all_to_all(a, axes, 0, 0, tiled=True)]
    ppermute x0 -> x9, starting transfers between devices: none -> 18.9 us  [shift(): return lax.ppermute(a, axis, pairs)]
    ppermute x0 -> x9, waiting for transfers between devices: none -> 13.2 us  [shift(): return lax.ppermute(a, axis, pairs)]
    all_to_all x6 -> x3, starting transfers between devices: 38.6 us -> 28.1 us  [exchange(): return lax.all_to_all(a, axes, 0, 0, tiled=True)]
    ppermute x5 -> x6, starting transfers between devices: 15 us -> 25.5 us  [swap(): return lax.ppermute(a, axes, [(n, n ^ flip) for n in range(size)])]
    pallas_call x5 -> x6, Pallas kernels: 16 us -> 22 us  [the longest x1 8.63 us: body(): call(flash_kernel, [shape((rows_a + 8, 256), BF)] * 4, scratch=[pltpu.VME...]
  transfers between devices with their start and end apart: 11 -> 18, of which waited for: 7 -> 10; matrix products, arithmetic and copies ran while one was open for 1% -> 0% of each run, Pallas kernels for 13% -> 13%
where the time goes in v2:
time: 208 us; the launch traced here: 206 us
  starting transfers between devices  72.5 us (35%)
  waiting for transfers between devices  55.5 us (27%)
  blocking collectives  35.2 us (17%)
  Pallas kernels  34 us (16%)
  local copies, waits for them, and re-layouts  7.63 us (4%)
    all_to_all x1, blocking collectives, exchange(): return lax.all_to_all(a, axes, 0, 0, tiled=True)  35.2 us
    all_to_all x3, starting transfers between devices, exchange(): return lax.all_to_all(a, axes, 0, 0, tiled=True)  28.1 us
    ppermute x6, waiting for transfers between devices, swap(): return lax.ppermute(a, axes, [(n, n ^ flip) for n in range(size)])  27 us
    ppermute x6, starting transfers between devices, swap(): return lax.ppermute(a, axes, [(n, n ^ flip) for n in range(size)])  25.5 us
    ppermute x9, starting transfers between devices, shift(): return lax.ppermute(a, axis, pairs)  18.9 us
    all_to_all x3, waiting for transfers between devices, exchange(): return lax.all_to_all(a, axes, 0, 0, tiled=True)  15.3 us
    ppermute x9, waiting for transfers between devices, shift(): return lax.ppermute(a, axis, pairs)  13.2 us
    pallas_call x1, Pallas kernels, body(): call(flash_kernel, [shape((rows_a + 8, 256), BF)] * 4, scratch=[pltpu.VME...  8.63 us
  transfers between devices with their start and end apart: 18, of which 10 were waited for; matrix products, arithmetic and copies ran while one was open for 0% of the time, Pallas kernels for 13%

profile of v2, /device:TPU:1, one launch (start us, length us, event | category | flops | bytes accessed | tf_op | source)
XLA Modules:
  0.0 206.5 jit_solution(15998369916914451418)
XLA Ops:
  3.0 4.0 %collective-permute-start.13 = (bf16[3,2048,128]{2,1,0:T(8,128)(2,1)S(1)}, bf16[3,2048,128]{2,1,0:T(8,128)(2,1)S(1)}, u32[]{:S(2)}, u32[]{:S(2)}) collective-permute-start(bf16[3,2048,128]{2,1,0:T(8,128)(2,1)S(1)} %constant_dynamic-update-slice_fusion.2.refs_0_.refs_1_), channel_id=1, source_target_pairs={{0,2},{2,0},{1,3},{3,1},{4,6},{6,4},{5,7},{7,5},{8,10},{10,8},{9,1... | collective-permute-start | bytes 4718600 | tf_op jit(solution)/shard_map/ppermute | solution.py:251
  7.0 6.6 %collective-permute-start.12 = (bf16[3,2048,128]{2,1,0:T(8,128)(2,1)S(1)}, bf16[3,2048,128]{2,1,0:T(8,128)(2,1)}, u32[]{:S(2)}, u32[]{:S(2)}) collective-permute-start(bf16[3,2048,128]{2,1,0:T(8,128)(2,1)S(1)} %constant_dynamic-update-slice_fusion.2.refs_0_.refs_1_), channel_id=1, source_target_pairs={{0,1},{1,0},{2,3},{3,2},{4,5},{5,4},{6,7},{7,6},{8,9},{9,8},{10,11... | collective-permute-start | bytes 4718600 | tf_op jit(solution)/shard_map/ppermute | solution.py:251
  13.7 22.6 %collective-permute-done.13.refs_4_.refs_5_.refs_2_ = bf16[3,2048,128]{2,1,0:T(8,128)(2,1)S(1)} collective-permute-done((bf16[3,2048,128]{2,1,0:T(8,128)(2,1)S(1)}, bf16[3,2048,128]{2,1,0:T(8,128)(2,1)S(1)}, u32[]{:S(2)}, u32[]{:S(2)}) %collective-permute-start.13) | collective-permute-done | bytes 1572896 | tf_op jit(solution)/shard_map/ppermute | solution.py:251
  36.3 8.0 %collective-permute-start.14 = (bf16[3,2048,128]{2,1,0:T(8,128)(2,1)S(1)}, bf16[3,2048,128]{2,1,0:T(8,128)(2,1)}, u32[]{:S(2)}, u32[]{:S(2)}) collective-permute-start(bf16[3,2048,128]{2,1,0:T(8,128)(2,1)S(1)} %collective-permute-done.13.refs_4_.refs_5_.refs_2_), channel_id=1, source_target_pairs={{0,1},{1,0},{2,3},{3,2},{4,5},{5,4},{6,7},{7,6},{8,9},{9,8},{10,11... | collective-permute-start | bytes 4718600 | tf_op jit(solution)/shard_map/ppermute | solution.py:251
  44.3 3.5 %shard_map.181 = bf16[32,24,512]{2,1,0:T(8,128)(2,1)} custom-call(bf16[128,2048]{1,0:T(8,128)(2,1)} %x_ref.3, f32[1,2048]{1,0:T(1,128)} %bitcast.9, s32[4,128]{1,0:T(4,128)} %bitcast.11), custom_call_target="tpu_custom_call" | custom-call | tf_op jit(solution)/shard_map/pallas_call | solution.py:286
  47.8 35.2 %all_to_all.20.in_ref = bf16[32,24,512]{2,1,0:T(8,128)(2,1)} all-to-all(bf16[32,24,512]{2,1,0:T(8,128)(2,1)} %shard_map.181), channel_id=1, replica_groups=mesh['w'=4,'v'=2,'x'=4,'g'=4,'r'=2,'c'=2] {'w','v','x'}, dimensions={0} | all-to-all | bytes 1572864 | tf_op jit(solution)/shard_map/all_to_all | solution.py:247
  83.0 5.7 %shard_map.182 = bf16[4,4,192,128]{3,2,1,0:T(8,128)(2,1)} custom-call(bf16[32,24,512]{2,1,0:T(8,128)(2,1)} %all_to_all.20.in_ref, bf16[3,2048,128]{2,1,0:T(8,128)(2,1)} %copy-done, bf16[3,2048,128]{2,1,0:T(8,128)(2,1)} %copy-done, bf16[3,2048,128]{2,1,0:T(8,128)(2,1)} %collective-permute-done.12.refs_2_.refs_3_.refs_1_, ...), custom_call_target="tpu_custom_call" | custom-call | tf_op jit(solution)/shard_map/pallas_call | solution.py:311
  88.7 6.8 %all-to-all-start.2 = ((bf16[4,4,192,128]{3,2,1,0:T(8,128)(2,1)}), bf16[4,4,192,128]{3,2,1,0:T(8,128)(2,1)S(1)}, u32[]{:S(2)}, u32[]{:S(2)}) async-start(bf16[4,4,192,128]{3,2,1,0:T(8,128)(2,1)} %shard_map.182), calls=%async_computation.2 | async-start | bytes 1572864 | tf_op jit(solution)/shard_map/all_to_all | solution.py:247
  95.6 3.6 %shard_map.176 = (bf16[256,128]{1,0:T(8,128)(2,1)}, bf16[256,256]{1,0:T(8,128)(2,1)}) custom-call(bf16[256,2048]{1,0:T(8,128)(2,1)} %x_ref.2, f32[1,2048]{1,0:T(1,128)} %bitcast.10, bf16[2048,128]{1,0:T(8,128)(2,1)} %wq_ref.1, bf16[2048,128]{1,0:T(8,128)(2,1)} %wk_ref.1, bf16[2048,128]{1,0:T(8,128)(2,1)} %wv_ref.1, f32[1,64]{1,0:T(1,128)} %bitcast.15, ...), custom_call_target="tpu_custom_call" | custom-call | tf_op jit(solution)/shard_map/pallas_call | solution.py:291
  99.1 1.9 collective-permute-start.3
  102.0 3.4 %collective-permute-done.3 = bf16[256,256]{1,0:T(8,128)(2,1)S(1)} collective-permute-done((bf16[256,256]{1,0:T(8,128)(2,1)}, bf16[256,256]{1,0:T(8,128)(2,1)S(1)}, u32[]{:S(2)}, u32[]{:S(2)}) %collective-permute-start.3) | collective-permute-done | bytes 131104 | tf_op jit(solution)/shard_map/ppermute | solution.py:251
  105.4 2.9 %collective-permute-start.6 = (bf16[512,256]{1,0:T(8,128)(2,1)S(1)}, bf16[512,256]{1,0:T(8,128)(2,1)S(1)}, u32[]{:S(2)}, u32[]{:S(2)}) collective-permute-start(bf16[512,256]{1,0:T(8,128)(2,1)S(1)} %constant_dynamic-update-slice_fusion.refs_4_), channel_id=1, source_target_pairs={{0,16},{16,32},{32,48},{48,0},{1,17},{17,33},{33,49},{49,1},{2,18}... | collective-permute-start | bytes 786440 | tf_op jit(solution)/shard_map/ppermute | solution.py:256
  108.2 5.0 %collective-permute-start.5 = (bf16[512,256]{1,0:T(8,128)(2,1)S(1)}, bf16[512,256]{1,0:T(8,128)(2,1)S(1)}, u32[]{:S(2)}, u32[]{:S(2)}) collective-permute-start(bf16[512,256]{1,0:T(8,128)(2,1)S(1)} %constant_dynamic-update-slice_fusion.refs_4_), channel_id=1, source_target_pairs={{0,32},{16,48},{32,0},{48,16},{1,33},{17,49},{33,1},{49,17},{2,34}... | collective-permute-start | bytes 786440 | tf_op jit(solution)/shard_map/ppermute | solution.py:256
  113.3 3.1 %collective-permute-start.4 = (bf16[512,256]{1,0:T(8,128)(2,1)S(1)}, bf16[512,256]{1,0:T(8,128)(2,1)S(1)}, u32[]{:S(2)}, u32[]{:S(2)}) collective-permute-start(bf16[512,256]{1,0:T(8,128)(2,1)S(1)} %constant_dynamic-update-slice_fusion.refs_4_), channel_id=1, source_target_pairs={{0,48},{16,0},{32,16},{48,32},{1,49},{17,1},{33,17},{49,33},{2,50}... | collective-permute-start | bytes 786440 | tf_op jit(solution)/shard_map/ppermute | solution.py:256
  116.4 1.4 collective-permute-start.2
  119.1 4.7 %collective-permute-done.2.refs_3_ = bf16[256,128]{1,0:T(8,128)(2,1)S(1)} collective-permute-done((bf16[256,128]{1,0:T(8,128)(2,1)}, bf16[256,128]{1,0:T(8,128)(2,1)S(1)}, u32[]{:S(2)}, u32[]{:S(2)}) %collective-permute-start.2) | collective-permute-done | bytes 65568 | tf_op jit(solution)/shard_map/ppermute | solution.py:256
  125.2 1.9 collective-permute-done.1.refs_2_
  127.1 4.3 %collective-permute-done.refs_1_ = bf16[256,128]{1,0:T(8,128)(2,1)S(1)} collective-permute-done((bf16[256,128]{1,0:T(8,128)(2,1)}, bf16[256,128]{1,0:T(8,128)(2,1)S(1)}, u32[]{:S(2)}, u32[]{:S(2)}) %collective-permute-start) | collective-permute-done | bytes 65568 | tf_op jit(solution)/shard_map/ppermute | solution.py:256
  133.0 8.6 %shard_map.177 = (bf16[264,256]{1,0:T(8,128)(2,1)}, bf16[264,256]{1,0:T(8,128)(2,1)}, bf16[264,256]{1,0:T(8,128)(2,1)}, bf16[264,256]{1,0:T(8,128)(2,1)}) custom-call(bf16[256,128]{1,0:T(8,128)(2,1)} %get-tuple-element.10.refs_0_, bf16[256,128]{1,0:T(8,128)(2,1)} %copy-done.17, bf16[256,128]{1,0:T(8,128)(2,1)} %copy-done.16, bf16[256,128]{1,0:T(8,128)(2,1)} %copy-done.15, ...), custom_call_target="tpu_custom_call" | custom-call | tf_op jit(solution)/shard_map/pallas_call | solution.py:320
  144.2 1.3 collective-permute-start.9
  146.6 1.8 collective-permute-done.9.refs_3_
  149.1 2.4 %shard_map.178 = bf16[16,128,128]{2,1,0:T(8,128)(2,1)} custom-call(f32[1]{0:T(128)S(6)} %copy.22.lam_ref, bf16[264,256]{1,0:T(8,128)(2,1)} %get-tuple-element.12.refs_0_, bf16[264,256]{1,0:T(8,128)(2,1)} %copy-done.12, bf16[264,256]{1,0:T(8,128)(2,1)} %copy-done.13, bf16[264,256]{1,0:T(8,128)(2,1)} %copy-done.14, f32[1,128]{1,0:T(1,128)} %bitcast.14), custom_call_target="tpu_custom_call" | custom-call | tf_op jit(solution)/shard_map/pallas_call | solution.py:339
  151.5 14.1 %all-to-all-start = ((bf16[16,128,128]{2,1,0:T(8,128)(2,1)}), bf16[16,128,128]{2,1,0:T(8,128)(2,1)S(1)}, u32[]{:S(2)}, u32[]{:S(2)}) async-start(bf16[16,128,128]{2,1,0:T(8,128)(2,1)} %shard_map.178), calls=%async_computation | async-start | bytes 1048576 | tf_op jit(solution)/shard_map/all_to_all | solution.py:247
  165.5 2.2 %collective-permute-start.10 = (bf16[2048,128]{1,0:T(8,128)(2,1)S(1)}, bf16[2048,128]{1,0:T(8,128)(2,1)S(1)}, u32[]{:S(2)}, u32[]{:S(2)}) collective-permute-start(bf16[2048,128]{1,0:T(8,128)(2,1)S(1)} %copy-done.6), channel_id=1, source_target_pairs={{0,1},{1,0},{2,3},{3,2},{4,5},{5,4},{6,7},{7,6},{8,9},{9,8},{10,11... | collective-permute-start | bytes 1572872 | tf_op jit(solution)/shard_map/ppermute | solution.py:251
  167.7 4.2 %shard_map.183 = bf16[32,4,8,128]{3,2,1,0:T(8,128)(2,1)} custom-call(bf16[4,4,192,128]{3,2,1,0:T(8,128)(2,1)} %copy-done.2, bf16[3,2048,128]{2,1,0:T(8,128)(2,1)} %copy-done, bf16[3,2048,128]{2,1,0:T(8,128)(2,1)} %collective-permute-done.12.refs_2_.refs_3_.refs_1_, bf16[3,2048,128]{2,1,0:T(8,128)(2,1)} %copy-done.1, ...), custom_call_target="tpu_custom_call" | custom-call | tf_op jit(solution)/shard_map/pallas_call | solution.py:329
  171.9 10.8 %all-to-all-done.rows_ref = bf16[16,128,128]{2,1,0:T(8,128)(2,1)S(1)} async-done(((bf16[16,128,128]{2,1,0:T(8,128)(2,1)}), bf16[16,128,128]{2,1,0:T(8,128)(2,1)S(1)}, u32[]{:S(2)}, u32[]{:S(2)}) %all-to-all-start) | async-done | bytes 524320 | tf_op jit(solution)/shard_map/all_to_all | solution.py:247
  182.7 7.2 %all-to-all-start.3 = ((bf16[128,8,128]{2,1,0:T(8,128)(2,1)}), bf16[128,8,128]{2,1,0:T(8,128)(2,1)S(1)}, u32[]{:S(2)}, u32[]{:S(2)}) async-start(bf16[128,8,128]{2,1,0:T(8,128)(2,1)} %bitcast.8), calls=%async_computation.3 | async-start | bytes 524288 | tf_op jit(solution)/shard_map/all_to_all | solution.py:247
  190.8 2.4 %shard_map.179 = (bf16[256,128]{1,0:T(8,128)(2,1)}, bf16[128,128]{1,0:T(8,128)(2,1)}) custom-call(bf16[16,128,128]{2,1,0:T(8,128)(2,1)} %copy-done.3, bf16[2048,128]{1,0:T(8,128)(2,1)} %own_ref.1, bf16[2048,128]{1,0:T(8,128)(2,1)} %copy-done.7), custom_call_target="tpu_custom_call" | custom-call | tf_op jit(solution)/shard_map/pallas_call | solution.py:343
  193.2 2.8 %collective-permute-start.11 = (bf16[128,128]{1,0:T(8,128)(2,1)}, bf16[128,128]{1,0:T(8,128)(2,1)S(1)}, u32[]{:S(2)}, u32[]{:S(2)}) collective-permute-start(bf16[128,128]{1,0:T(8,128)(2,1)} %get-tuple-element.17), channel_id=1, source_target_pairs={{0,1},{1,0},{2,3},{3,2},{4,5},{5,4},{6,7},{7,6},{8,9},{9,8},{10,11... | collective-permute-start | bytes 98312 | tf_op jit(solution)/shard_map/ppermute | solution.py:251
  197.7 1.5 shard_map.180
  199.2 4.5 %all-to-all-done.3.rows_ref = bf16[128,8,128]{2,1,0:T(8,128)(2,1)S(1)} async-done(((bf16[128,8,128]{2,1,0:T(8,128)(2,1)}), bf16[128,8,128]{2,1,0:T(8,128)(2,1)S(1)}, u32[]{:S(2)}, u32[]{:S(2)}) %all-to-all-start.3) | async-done | bytes 262176 | tf_op jit(solution)/shard_map/all_to_all | solution.py:247
  204.3 2.2 %shard_map.184 = bf16[128,128]{1,0:T(8,128)(2,1)} custom-call(s32[4,128]{1,0:T(4,128)} %bitcast.12, f32[4,128]{1,0:T(4,128)} %bitcast.13, bf16[128,8,128]{2,1,0:T(8,128)(2,1)} %copy-done.4), custom_call_target="tpu_custom_call" | custom-call | tf_op jit(solution)/shard_map/pallas_call | solution.py:354
  (57 shorter events, 14.3 us)
Async XLA Ops:
  0.6 2.3 %copy-start.8 = (bf16[1,2048,128]{2,1,0:T(8,128)(2,1)S(1)}, bf16[1,2048,128]{2,1,0:T(8,128)(2,1)}, u32[]{:S(2)}) copy-start(bf16[1,2048,128]{2,1,0:T(8,128)(2,1)} %param.33) | copy-start | bytes 1572868
  3.0 80.1 %copy-start = (bf16[3,2048,128]{2,1,0:T(8,128)(2,1)}, bf16[3,2048,128]{2,1,0:T(8,128)(2,1)S(1)}, u32[]{:S(2)}) copy-start(bf16[3,2048,128]{2,1,0:T(8,128)(2,1)S(1)} %constant_dynamic-update-slice_fusion.2.refs_0_.refs_1_) | copy-start | bytes 4718596
  3.0 33.3 %collective-permute-start.13 = (bf16[3,2048,128]{2,1,0:T(8,128)(2,1)S(1)}, bf16[3,2048,128]{2,1,0:T(8,128)(2,1)S(1)}, u32[]{:S(2)}, u32[]{:S(2)}) collective-permute-start(bf16[3,2048,128]{2,1,0:T(8,128)(2,1)S(1)} %constant_dynamic-update-slice_fusion.2.refs_0_.refs_1_), channel_id=1, source_target_pairs={{0,2},{2,0},{1,3},{3,1},{4,6},{6,4},{5,7},{7,5},{8,10},{10,8},{9,1... | collective-permute-start | bytes 4718600 | tf_op jit(solution)/shard_map/ppermute | solution.py:251
  7.0 76.0 %collective-permute-start.12 = (bf16[3,2048,128]{2,1,0:T(8,128)(2,1)S(1)}, bf16[3,2048,128]{2,1,0:T(8,128)(2,1)}, u32[]{:S(2)}, u32[]{:S(2)}) collective-permute-start(bf16[3,2048,128]{2,1,0:T(8,128)(2,1)S(1)} %constant_dynamic-update-slice_fusion.2.refs_0_.refs_1_), channel_id=1, source_target_pairs={{0,1},{1,0},{2,3},{3,2},{4,5},{5,4},{6,7},{7,6},{8,9},{9,8},{10,11... | collective-permute-start | bytes 4718600 | tf_op jit(solution)/shard_map/ppermute | solution.py:251
  36.3 46.7 %copy-start.1 = (bf16[3,2048,128]{2,1,0:T(8,128)(2,1)}, bf16[3,2048,128]{2,1,0:T(8,128)(2,1)S(1)}, u32[]{:S(2)}) copy-start(bf16[3,2048,128]{2,1,0:T(8,128)(2,1)S(1)} %collective-permute-done.13.refs_4_.refs_5_.refs_2_) | copy-start | bytes 4718596
  36.3 46.7 %collective-permute-start.14 = (bf16[3,2048,128]{2,1,0:T(8,128)(2,1)S(1)}, bf16[3,2048,128]{2,1,0:T(8,128)(2,1)}, u32[]{:S(2)}, u32[]{:S(2)}) collective-permute-start(bf16[3,2048,128]{2,1,0:T(8,128)(2,1)S(1)} %collective-permute-done.13.refs_4_.refs_5_.refs_2_), channel_id=1, source_target_pairs={{0,1},{1,0},{2,3},{3,2},{4,5},{5,4},{6,7},{7,6},{8,9},{9,8},{10,11... | collective-permute-start | bytes 4718600 | tf_op jit(solution)/shard_map/ppermute | solution.py:251
  88.7 62.7 %all-to-all-start.2 = ((bf16[4,4,192,128]{3,2,1,0:T(8,128)(2,1)}), bf16[4,4,192,128]{3,2,1,0:T(8,128)(2,1)S(1)}, u32[]{:S(2)}, u32[]{:S(2)}) async-start(bf16[4,4,192,128]{3,2,1,0:T(8,128)(2,1)} %shard_map.182), calls=%async_computation.2 | async-start | bytes 1572864 | tf_op jit(solution)/shard_map/all_to_all | solution.py:247
  99.1 6.2 %collective-permute-start.3 = (bf16[256,256]{1,0:T(8,128)(2,1)}, bf16[256,256]{1,0:T(8,128)(2,1)S(1)}, u32[]{:S(2)}, u32[]{:S(2)}) collective-permute-start(bf16[256,256]{1,0:T(8,128)(2,1)} %get-tuple-element.11), channel_id=1, source_target_pairs={{0,64},{64,0},{1,65},{65,1},{2,66},{66,2},{3,67},{67,3},{4,68},{68... | collective-permute-start | bytes 393224 | tf_op jit(solution)/shard_map/ppermute | solution.py:251
  105.4 26.0 %copy-start.5 = (bf16[512,256]{1,0:T(8,128)(2,1)}, bf16[512,256]{1,0:T(8,128)(2,1)S(1)}, u32[]{:S(2)}) copy-start(bf16[512,256]{1,0:T(8,128)(2,1)S(1)} %constant_dynamic-update-slice_fusion.refs_4_) | copy-start | bytes 786436
  105.4 26.0 %collective-permute-start.6 = (bf16[512,256]{1,0:T(8,128)(2,1)S(1)}, bf16[512,256]{1,0:T(8,128)(2,1)S(1)}, u32[]{:S(2)}, u32[]{:S(2)}) collective-permute-start(bf16[512,256]{1,0:T(8,128)(2,1)S(1)} %constant_dynamic-update-slice_fusion.refs_4_), channel_id=1, source_target_pairs={{0,16},{16,32},{32,48},{48,0},{1,17},{17,33},{33,49},{49,1},{2,18}... | collective-permute-start | bytes 786440 | tf_op jit(solution)/shard_map/ppermute | solution.py:256
  108.2 23.1 %collective-permute-start.5 = (bf16[512,256]{1,0:T(8,128)(2,1)S(1)}, bf16[512,256]{1,0:T(8,128)(2,1)S(1)}, u32[]{:S(2)}, u32[]{:S(2)}) collective-permute-start(bf16[512,256]{1,0:T(8,128)(2,1)S(1)} %constant_dynamic-update-slice_fusion.refs_4_), channel_id=1, source_target_pairs={{0,32},{16,48},{32,0},{48,16},{1,33},{17,49},{33,1},{49,17},{2,34}... | collective-permute-start | bytes 786440 | tf_op jit(solution)/shard_map/ppermute | solution.py:256
  113.3 18.1 %collective-permute-start.4 = (bf16[512,256]{1,0:T(8,128)(2,1)S(1)}, bf16[512,256]{1,0:T(8,128)(2,1)S(1)}, u32[]{:S(2)}, u32[]{:S(2)}) collective-permute-start(bf16[512,256]{1,0:T(8,128)(2,1)S(1)} %constant_dynamic-update-slice_fusion.refs_4_), channel_id=1, source_target_pairs={{0,48},{16,0},{32,16},{48,32},{1,49},{17,1},{33,17},{49,33},{2,50}... | collective-permute-start | bytes 786440 | tf_op jit(solution)/shard_map/ppermute | solution.py:256
  116.4 49.1 %copy-start.6 = (bf16[2048,128]{1,0:T(8,128)(2,1)S(1)}, bf16[2048,128]{1,0:T(8,128)(2,1)}, u32[]{:S(2)}) copy-start(bf16[2048,128]{1,0:T(8,128)(2,1)} %own_ref.1) | copy-start | bytes 1572868
  116.4 7.5 %collective-permute-start.2 = (bf16[256,128]{1,0:T(8,128)(2,1)}, bf16[256,128]{1,0:T(8,128)(2,1)S(1)}, u32[]{:S(2)}, u32[]{:S(2)}) collective-permute-start(bf16[256,128]{1,0:T(8,128)(2,1)} %get-tuple-element.10.refs_0_), channel_id=1, source_target_pairs={{384,0},{385,1},{386,2},{387,3},{388,4},{389,5},{390,6},{391,7},{3... | collective-permute-start | bytes 196616 | tf_op jit(solution)/shard_map/ppermute | solution.py:256
  117.8 9.2 %collective-permute-start.1 = (bf16[256,128]{1,0:T(8,128)(2,1)}, bf16[256,128]{1,0:T(8,128)(2,1)S(1)}, u32[]{:S(2)}, u32[]{:S(2)}) collective-permute-start(bf16[256,128]{1,0:T(8,128)(2,1)} %get-tuple-element.10.refs_0_), channel_id=1, source_target_pairs={{256,0},{384,128},{257,1},{385,129},{258,2},{386,130},{259,3},{387... | collective-permute-start | bytes 196616 | tf_op jit(solution)/shard_map/ppermute | solution.py:256
  123.9 7.6 %copy-start.15 = (bf16[256,128]{1,0:T(8,128)(2,1)}, bf16[256,128]{1,0:T(8,128)(2,1)S(1)}, u32[]{:S(2)}) copy-start(bf16[256,128]{1,0:T(8,128)(2,1)S(1)} %collective-permute-done.2.refs_3_) | copy-start | bytes 196612
  123.9 7.5 %collective-permute-start = (bf16[256,128]{1,0:T(8,128)(2,1)}, bf16[256,128]{1,0:T(8,128)(2,1)S(1)}, u32[]{:S(2)}, u32[]{:S(2)}) collective-permute-start(bf16[256,128]{1,0:T(8,128)(2,1)} %get-tuple-element.10.refs_0_), channel_id=1, source_target_pairs={{128,0},{256,128},{384,256},{129,1},{257,129},{385,257},{130,2},{2... | collective-permute-start | bytes 196616 | tf_op jit(solution)/shard_map/ppermute | solution.py:256
  127.1 4.4 %copy-start.16 = (bf16[256,128]{1,0:T(8,128)(2,1)}, bf16[256,128]{1,0:T(8,128)(2,1)S(1)}, u32[]{:S(2)}) copy-start(bf16[256,128]{1,0:T(8,128)(2,1)S(1)} %collective-permute-done.1.refs_2_) | copy-start | bytes 196612
  131.4 0.8 copy-start.9
  131.4 0.9 copy-start.10
  141.6 4.6 %collective-permute-start.7 = (bf16[264,256]{1,0:T(8,128)(2,1)}, bf16[264,256]{1,0:T(8,128)(2,1)S(1)}, u32[]{:S(2)}, u32[]{:S(2)}) collective-permute-start(bf16[264,256]{1,0:T(8,128)(2,1)} %get-tuple-element.13), channel_id=1, source_target_pairs={{0,128},{128,256},{256,384},{1,129},{129,257},{257,385},{2,130},{1... | collective-permute-start | bytes 405512 | tf_op jit(solution)/shard_map/ppermute | solution.py:256
  142.9 3.7 %collective-permute-start.8 = (bf16[264,256]{1,0:T(8,128)(2,1)}, bf16[264,256]{1,0:T(8,128)(2,1)S(1)}, u32[]{:S(2)}, u32[]{:S(2)}) collective-permute-start(bf16[264,256]{1,0:T(8,128)(2,1)} %get-tuple-element.14), channel_id=1, source_target_pairs={{0,256},{128,384},{1,257},{129,385},{2,258},{130,386},{3,259},{131... | collective-permute-start | bytes 405512 | tf_op jit(solution)/shard_map/ppermute | solution.py:256
  144.2 4.2 %collective-permute-start.9 = (bf16[264,256]{1,0:T(8,128)(2,1)}, bf16[264,256]{1,0:T(8,128)(2,1)S(1)}, u32[]{:S(2)}, u32[]{:S(2)}) collective-permute-start(bf16[264,256]{1,0:T(8,128)(2,1)} %get-tuple-element.15), channel_id=1, source_target_pairs={{0,384},{1,385},{2,386},{3,387},{4,388},{5,389},{6,390},{7,391},{8... | collective-permute-start | bytes 405512 | tf_op jit(solution)/shard_map/ppermute | solution.py:256
  146.2 2.3 %copy-start.12 = (bf16[264,256]{1,0:T(8,128)(2,1)}, bf16[264,256]{1,0:T(8,128)(2,1)S(1)}, u32[]{:S(2)}) copy-start(bf16[264,256]{1,0:T(8,128)(2,1)S(1)} %collective-permute-done.7.refs_1_) | copy-start | bytes 405508
  146.6 1.8 copy-start.13
  151.5 16.3 %copy-start.2 = (bf16[4,4,192,128]{3,2,1,0:T(8,128)(2,1)}, bf16[4,4,192,128]{3,2,1,0:T(8,128)(2,1)S(1)}, u32[]{:S(2)}) copy-start(bf16[4,4,192,128]{3,2,1,0:T(8,128)(2,1)S(1)} %all-to-all-done.2.hidden_ref) | copy-start | bytes 2359300
  151.5 31.3 %all-to-all-start = ((bf16[16,128,128]{2,1,0:T(8,128)(2,1)}), bf16[16,128,128]{2,1,0:T(8,128)(2,1)S(1)}, u32[]{:S(2)}, u32[]{:S(2)}) async-start(bf16[16,128,128]{2,1,0:T(8,128)(2,1)} %shard_map.178), calls=%async_computation | async-start | bytes 1048576 | tf_op jit(solution)/shard_map/all_to_all | solution.py:247
  165.5 24.4 %collective-permute-start.10 = (bf16[2048,128]{1,0:T(8,128)(2,1)S(1)}, bf16[2048,128]{1,0:T(8,128)(2,1)S(1)}, u32[]{:S(2)}, u32[]{:S(2)}) collective-permute-start(bf16[2048,128]{1,0:T(8,128)(2,1)S(1)} %copy-done.6), channel_id=1, source_target_pairs={{0,1},{1,0},{2,3},{3,2},{4,5},{5,4},{6,7},{7,6},{8,9},{9,8},{10,11... | collective-permute-start | bytes 1572872 | tf_op jit(solution)/shard_map/ppermute | solution.py:251
  182.7 7.2 %copy-start.3 = (bf16[16,128,128]{2,1,0:T(8,128)(2,1)}, bf16[16,128,128]{2,1,0:T(8,128)(2,1)S(1)}, u32[]{:S(2)}) copy-start(bf16[16,128,128]{2,1,0:T(8,128)(2,1)S(1)} %all-to-all-done.rows_ref) | copy-start | bytes 1572868
  182.7 20.9 %all-to-all-start.3 = ((bf16[128,8,128]{2,1,0:T(8,128)(2,1)}), bf16[128,8,128]{2,1,0:T(8,128)(2,1)S(1)}, u32[]{:S(2)}, u32[]{:S(2)}) async-start(bf16[128,8,128]{2,1,0:T(8,128)(2,1)} %bitcast.8), calls=%async_computation.3 | async-start | bytes 524288 | tf_op jit(solution)/shard_map/all_to_all | solution.py:247
  190.0 0.8 copy-start.7
  193.2 3.8 %collective-permute-start.11 = (bf16[128,128]{1,0:T(8,128)(2,1)}, bf16[128,128]{1,0:T(8,128)(2,1)S(1)}, u32[]{:S(2)}, u32[]{:S(2)}) collective-permute-start(bf16[128,128]{1,0:T(8,128)(2,1)} %get-tuple-element.17), channel_id=1, source_target_pairs={{0,1},{1,0},{2,3},{3,2},{4,5},{5,4},{6,7},{7,6},{8,9},{9,8},{10,11... | collective-permute-start | bytes 98312 | tf_op jit(solution)/shard_map/ppermute | solution.py:251
  (5 other events, 3.3 us)

commit v3 on v2

--- a/solution.py
+++ b/solution.py
@@ -93,64 +93,62 @@
         )
         return wide * scale * jnp.concatenate([gain, gain], axis=1)
 
-    q = (component_norm(dot(normed, wq_ref[...]), qg_ref[...]) * 0.125).astype(BF)
-    k = component_norm(dot(normed, wk_ref[...]), kg_ref[...]).astype(BF)
+    both = dot(normed, jnp.concatenate([wq_ref[...], wk_ref[...]], axis=1))
+    q = (component_norm(both[:, 0:128], qg_ref[...]) * 0.125).astype(BF)
+    k = component_norm(both[:, 128:256], kg_ref[...]).astype(BF)
     v = dot(normed, wv_ref[...]).astype(BF)
     q_ref[...] = q
     kv_ref[:, 0:128] = k
     kv_ref[:, 128:256] = v
 
 
-def flash_kernel(*refs):
-    q_refs, kv_refs, outs, total_ref, q_all = refs[0:4], refs[4:8], refs[8:12], refs[12], refs[13]
+def flash_kernel(steps, *refs):
+    size = len(steps)
+    q_refs, kv_refs, outs = refs[:size], refs[size : size + 4], refs[size + 4 : 2 * size + 4]
+    total_ref = refs[-1]
     w, v, x = (lax.axis_index(name) for name in EP)
     rows = q_refs[0].shape[0]
     keys = kv_refs[0].shape[0]
     half = keys // 2
     ones = jnp.ones((keys, 128), BF)
-    for n in range(4):
-        q_all[n] = q_refs[n][...]
-
-    def attend(n, masked):
-        for comp in range(2):
-            lanes = slice(64 * comp, 64 * comp + 64)
-            q = q_all[n, :, lanes]
-            total = None
-            for turn in range(4):
-                kv = kv_refs[turn][...]
-                value = jnp.concatenate([kv[:, 128:256], ones], axis=1)
-                weight = jnp.exp(dot(q, kv[:, lanes], ((1,), (1,))))
-                if masked:
-                    source = (x + turn) % 4
-                    first = 1024 * v + 256 * source
-                    second = 1024 * (1 - v) + 256 * source
-                    mine = 1024 * v + 256 * x
-                    col = lax.broadcasted_iota(jnp.int32, weight.shape, 1)
-                    row = lax.broadcasted_iota(jnp.int32, weight.shape, 0)
-                    key_pos = jnp.where(col < half, col + first, col - half + second)
-                    weight = jnp.where(key_pos <= row + mine, weight, 0.0)
-                piece = dot(weight.astype(BF), value)
-                total = piece if total is None else total + piece
-            total_ref[n, comp] = total
-
-    attend(0, True)
-
-    def later(n, carry):
-        attend(n, False)
-        return carry
-
-    lax.fori_loop(1, 4 - w, later, 0)
-    for n in range(4):
-
-        @pl.when(n + w < 4)
+
+    def attend(q_ref, comp, masked):
+        lanes = slice(64 * comp, 64 * comp + 64)
+        total = None
+        for turn in range(4):
+            kv = kv_refs[turn][...]
+            value = jnp.concatenate([kv[:, 128:256], ones], axis=1)
+            scores = dot(q_ref[:, lanes], kv[:, lanes], ((1,), (1,)))
+            weight = jnp.exp2(scores * 1.4426950408889634)
+            if masked:
+                source = (x + turn) % 4
+                first = 1024 * v + 256 * source
+                second = 1024 * (1 - v) + 256 * source
+                mine = 1024 * v + 256 * x
+                col = lax.broadcasted_iota(jnp.int32, weight.shape, 1)
+                row = lax.broadcasted_iota(jnp.int32, weight.shape, 0)
+                key_pos = jnp.where(col < half, col + first, col - half + second)
+                weight = jnp.where(key_pos <= row + mine, weight, 0.0)
+            piece = dot(weight.astype(BF), value)
+            total = piece if total is None else total + piece
+        total_ref[comp] = total
+
+    for n, step in enumerate(steps):
+
+        @pl.when(w + step < 4)
         def _():
             lines = []
             for comp in range(2):
-                outs[n][0:rows, 128 * comp : 128 * comp + 128] = total_ref[n, comp, :, 0:128].astype(BF)
-                sums = total_ref[n, comp, :, 128:256].T[0:1]
+                attend(q_refs[n], comp, step == 0)
+                outs[n][0:rows, 128 * comp : 128 * comp + 128] = total_ref[comp, :, 0:128].astype(BF)
+                sums = total_ref[comp, :, 128:256].T[0:1]
                 high = sums.astype(BF).astype(F32)
                 lines += [high, sums - high]
             outs[n][rows:, :] = jnp.concatenate(lines + [jnp.zeros((4, rows), F32)], axis=0).astype(BF)
+
+
+def partial_kernel(steps):
+    return lambda *refs: flash_kernel(steps, *refs)
 
 
 def mix_kernel(lam_ref, *refs):
@@ -175,8 +173,9 @@
     rows = jnp.concatenate([rows_ref[n] for n in range(rows_ref.shape[0])], axis=1)
     count = rows.shape[0]
     spot = pl.multiple_of(lax.axis_index("c") * count, count)
-    out_ref[pl.ds(spot, count), :] = dot(rows, own_ref[...]).astype(BF)
-    other_out[...] = dot(rows, other_ref[...]).astype(BF)
+    both = dot(rows, jnp.concatenate([own_ref[...], other_ref[...]], axis=1)).astype(BF)
+    out_ref[pl.ds(spot, count), :] = both[:, 0:128]
+    other_out[...] = both[:, 128:256]
 
 
 def finish_kernel(out_ref, received_ref, done_ref):
@@ -201,8 +200,9 @@
         pieces.append(dot(pick, flat).astype(BF))
     rows = jnp.concatenate(pieces, axis=1)
     for n in range(4):
-        gate = jnp.minimum(dot(rows, weights[2 * n][0]), 7.0)
-        up = jnp.clip(dot(rows, weights[2 * n + 1][0]), -7.0, 7.0)
+        both = dot(rows, jnp.concatenate([weights[2 * n][0], weights[2 * n + 1][0]], axis=1))
+        gate = jnp.minimum(both[:, 0:128], 7.0)
+        up = jnp.clip(both[:, 128:256], -7.0, 7.0)
         hidden = (gate * jax.nn.sigmoid(1.702 * gate) * (up + 1.0)).astype(BF)
         for peer in range(out_ref.shape[0]):
             out_ref[peer, place ^ n] = hidden
@@ -220,10 +220,12 @@
     line = lax.broadcasted_iota(jnp.int32, (sources * 8, count), 1)
     hit = ((wide // 8) * 6 + wide % 8 == line) & (wide % 8 < 6)
     pick = jnp.where(hit, 1.0, 0.0).astype(BF)
-    for n in range(4):
-        result = dot(rows, weights[n][0]).astype(BF)
-        result = dot(pick, result).astype(BF)
-        out_ref[:, place ^ n] = result.reshape(sources, 8, result.shape[1])
+    for pair in range(2):
+        wide_weight = jnp.concatenate([weights[2 * pair][0], weights[2 * pair + 1][0]], axis=1)
+        result = dot(pick, dot(rows, wide_weight).astype(BF)).astype(BF)
+        for n in range(2):
+            piece = result[:, 128 * n : 128 * n + 128]
+            out_ref[:, place ^ (2 * pair + n)] = piece.reshape(sources, 8, 128)
 
 
 def combine_kernel(routes_ref, weight_ref, rows_ref, out_ref):
@@ -317,13 +319,17 @@
     )(incoming, *[w for w in quad for _ in range(2)])
     hidden_all = exchange(hidden, "g")
 
-    partial = call(
-        flash_kernel,
-        [shape((rows_a + 8, 256), BF)] * 4,
-        scratch=[pltpu.VMEM((4, 2, rows_a, 256), F32), pltpu.VMEM((4, rows_a, 128), BF)],
-        smem_first=False,
-        count=8,
-    )(*q_all, *kv_all)
+    partial = [None] * 4
+    for steps in GROUPS:
+        outs = call(
+            partial_kernel(steps),
+            [shape((rows_a + 8, 256), BF)] * len(steps),
+            scratch=[pltpu.VMEM((2, rows_a, 256), F32)],
+            smem_first=False,
+            count=len(steps) + 4,
+        )(*[q_all[n] for n in steps], *kv_all)
+        for n, out in zip(steps, outs):
+            partial[n] = out
     partial_all = [partial[0]] + [shift(partial[n], "w", 4, n, False) for n in range(1, 4)]
 
     result = pl.pallas_call(
@@ -357,6 +363,9 @@
     return (attn_out, moe_out)
 
 
+GROUPS = ((3, 2, 1), (0,))
+
+
 def solution(mesh):
     finer = Mesh(mesh.devices.reshape(4, 2, 4, 4, 2, 2), EP + TP)
     placed = (

time: 208 us -> 204 us (0.981)
    ppermute x9, waiting for transfers between devices: 13.2 us -> 11.1 us  [shift(): return lax.ppermute(a, axis, pairs)]
    pallas_call x1 -> x2, Pallas kernels: 8.63 us -> 10.2 us  [body(): call(partial_kernel(steps), [shape((rows_a + 8, 256), BF)] * len(steps),...]
  transfers between devices with their start and end apart: 18 -> 18, of which waited for: 10 -> 8; matrix products, arithmetic and copies ran while one was open for 0% -> 0% of each run, Pallas kernels for 13% -> 13%
where the time goes in v3:
time: 204 us; the launch traced here: 203 us
  starting transfers between devices  70.7 us (35%)
  waiting for transfers between devices  53.8 us (26%)
  blocking collectives  35.2 us (17%)
  Pallas kernels  34.3 us (17%)
  local copies, waits for them, and re-layouts  7.72 us (4%)
    all_to_all x1, blocking collectives, exchange(): return lax.all_to_all(a, axes, 0, 0, tiled=True)  35.2 us
    ppermute x6, waiting for transfers between devices, swap(): return lax.ppermute(a, axes, [(n, n ^ flip) for n in range(size)])  27 us
    all_to_all x3, starting transfers between devices, exchange(): return lax.all_to_all(a, axes, 0, 0, tiled=True)  26.5 us
    ppermute x6, starting transfers between devices, swap(): return lax.ppermute(a, axes, [(n, n ^ flip) for n in range(size)])  25.5 us
    ppermute x9, starting transfers between devices, shift(): return lax.ppermute(a, axis, pairs)  18.7 us
    all_to_all x3, waiting for transfers between devices, exchange(): return lax.all_to_all(a, axes, 0, 0, tiled=True)  15.7 us
    ppermute x9, waiting for transfers between devices, shift(): return lax.ppermute(a, axis, pairs)  11.1 us
    pallas_call x2, Pallas kernels, body(): call(partial_kernel(steps), [shape((rows_a + 8, 256), BF)] * len(steps),...  10.2 us
  transfers between devices with their start and end apart: 18, of which 8 were waited for; matrix products, arithmetic and copies ran while one was open for 0% of the time, Pallas kernels for 13%

profile of v3, /device:TPU:1, one launch (start us, length us, event | category | flops | bytes accessed | tf_op | source)
XLA Modules:
  0.0 203.4 jit_solution(6494419600166452759)
XLA Ops:
  3.0 4.0 %collective-permute-start.13 = (bf16[3,2048,128]{2,1,0:T(8,128)(2,1)S(1)}, bf16[3,2048,128]{2,1,0:T(8,128)(2,1)S(1)}, u32[]{:S(2)}, u32[]{:S(2)}) collective-permute-start(bf16[3,2048,128]{2,1,0:T(8,128)(2,1)S(1)} %constant_dynamic-update-slice_fusion.2.refs_0_.refs_1_), channel_id=1, source_target_pairs={{0,2},{2,0},{1,3},{3,1},{4,6},{6,4},{5,7},{7,5},{8,10},{10,8},{9,1... | collective-permute-start | bytes 4718600 | tf_op jit(solution)/shard_map/ppermute | solution.py:253
  7.0 6.6 %collective-permute-start.12 = (bf16[3,2048,128]{2,1,0:T(8,128)(2,1)S(1)}, bf16[3,2048,128]{2,1,0:T(8,128)(2,1)}, u32[]{:S(2)}, u32[]{:S(2)}) collective-permute-start(bf16[3,2048,128]{2,1,0:T(8,128)(2,1)S(1)} %constant_dynamic-update-slice_fusion.2.refs_0_.refs_1_), channel_id=1, source_target_pairs={{0,1},{1,0},{2,3},{3,2},{4,5},{5,4},{6,7},{7,6},{8,9},{9,8},{10,11... | collective-permute-start | bytes 4718600 | tf_op jit(solution)/shard_map/ppermute | solution.py:253
  13.7 22.6 %collective-permute-done.13.refs_4_.refs_5_.refs_2_ = bf16[3,2048,128]{2,1,0:T(8,128)(2,1)S(1)} collective-permute-done((bf16[3,2048,128]{2,1,0:T(8,128)(2,1)S(1)}, bf16[3,2048,128]{2,1,0:T(8,128)(2,1)S(1)}, u32[]{:S(2)}, u32[]{:S(2)}) %collective-permute-start.13) | collective-permute-done | bytes 1572896 | tf_op jit(solution)/shard_map/ppermute | solution.py:253
  36.3 8.0 %collective-permute-start.14 = (bf16[3,2048,128]{2,1,0:T(8,128)(2,1)S(1)}, bf16[3,2048,128]{2,1,0:T(8,128)(2,1)}, u32[]{:S(2)}, u32[]{:S(2)}) collective-permute-start(bf16[3,2048,128]{2,1,0:T(8,128)(2,1)S(1)} %collective-permute-done.13.refs_4_.refs_5_.refs_2_), channel_id=1, source_target_pairs={{0,1},{1,0},{2,3},{3,2},{4,5},{5,4},{6,7},{7,6},{8,9},{9,8},{10,11... | collective-permute-start | bytes 4718600 | tf_op jit(solution)/shard_map/ppermute | solution.py:253
  44.3 3.5 %shard_map.182 = bf16[32,24,512]{2,1,0:T(8,128)(2,1)} custom-call(bf16[128,2048]{1,0:T(8,128)(2,1)} %x_ref.3, f32[1,2048]{1,0:T(1,128)} %bitcast.9, s32[4,128]{1,0:T(4,128)} %bitcast.11), custom_call_target="tpu_custom_call" | custom-call | tf_op jit(solution)/shard_map/pallas_call | solution.py:288
  47.8 35.2 %all_to_all.20.in_ref = bf16[32,24,512]{2,1,0:T(8,128)(2,1)} all-to-all(bf16[32,24,512]{2,1,0:T(8,128)(2,1)} %shard_map.182), channel_id=1, replica_groups=mesh['w'=4,'v'=2,'x'=4,'g'=4,'r'=2,'c'=2] {'w','v','x'}, dimensions={0} | all-to-all | bytes 1572864 | tf_op jit(solution)/shard_map/all_to_all | solution.py:249
  83.0 4.9 %shard_map.183 = bf16[4,4,192,128]{3,2,1,0:T(8,128)(2,1)} custom-call(bf16[32,24,512]{2,1,0:T(8,128)(2,1)} %all_to_all.20.in_ref, bf16[3,2048,128]{2,1,0:T(8,128)(2,1)} %copy-done, bf16[3,2048,128]{2,1,0:T(8,128)(2,1)} %copy-done, bf16[3,2048,128]{2,1,0:T(8,128)(2,1)} %collective-permute-done.12.refs_2_.refs_3_.refs_1_, ...), custom_call_target="tpu_custom_call" | custom-call | tf_op jit(solution)/shard_map/pallas_call | solution.py:313
  88.0 6.8 %all-to-all-start.2 = ((bf16[4,4,192,128]{3,2,1,0:T(8,128)(2,1)}), bf16[4,4,192,128]{3,2,1,0:T(8,128)(2,1)S(1)}, u32[]{:S(2)}, u32[]{:S(2)}) async-start(bf16[4,4,192,128]{3,2,1,0:T(8,128)(2,1)} %shard_map.183), calls=%async_computation.2 | async-start | bytes 1572864 | tf_op jit(solution)/shard_map/all_to_all | solution.py:249
  94.8 3.5 %shard_map.176 = (bf16[256,128]{1,0:T(8,128)(2,1)}, bf16[256,256]{1,0:T(8,128)(2,1)}) custom-call(bf16[256,2048]{1,0:T(8,128)(2,1)} %x_ref.2, f32[1,2048]{1,0:T(1,128)} %bitcast.10, bf16[2048,128]{1,0:T(8,128)(2,1)} %wq_ref.1, bf16[2048,128]{1,0:T(8,128)(2,1)} %wk_ref.1, bf16[2048,128]{1,0:T(8,128)(2,1)} %wv_ref.1, f32[1,64]{1,0:T(1,128)} %bitcast.15, ...), custom_call_target="tpu_custom_call" | custom-call | tf_op jit(solution)/shard_map/pallas_call | solution.py:293
  98.3 1.9 collective-permute-start
  101.1 3.4 %collective-permute-done = bf16[256,256]{1,0:T(8,128)(2,1)S(1)} collective-permute-done((bf16[256,256]{1,0:T(8,128)(2,1)}, bf16[256,256]{1,0:T(8,128)(2,1)S(1)}, u32[]{:S(2)}, u32[]{:S(2)}) %collective-permute-start) | collective-permute-done | bytes 131104 | tf_op jit(solution)/shard_map/ppermute | solution.py:253
  104.5 2.9 %collective-permute-start.3 = (bf16[512,256]{1,0:T(8,128)(2,1)S(1)}, bf16[512,256]{1,0:T(8,128)(2,1)S(1)}, u32[]{:S(2)}, u32[]{:S(2)}) collective-permute-start(bf16[512,256]{1,0:T(8,128)(2,1)S(1)} %constant_dynamic-update-slice_fusion.refs_1_.refs_3_), channel_id=1, source_target_pairs={{0,16},{16,32},{32,48},{48,0},{1,17},{17,33},{33,49},{49,1},{2,18}... | collective-permute-start | bytes 786440 | tf_op jit(solution)/shard_map/ppermute | solution.py:258
  107.4 5.1 %collective-permute-start.2 = (bf16[512,256]{1,0:T(8,128)(2,1)S(1)}, bf16[512,256]{1,0:T(8,128)(2,1)S(1)}, u32[]{:S(2)}, u32[]{:S(2)}) collective-permute-start(bf16[512,256]{1,0:T(8,128)(2,1)S(1)} %constant_dynamic-update-slice_fusion.refs_1_.refs_3_), channel_id=1, source_target_pairs={{0,32},{16,48},{32,0},{48,16},{1,33},{17,49},{33,1},{49,17},{2,34}... | collective-permute-start | bytes 786440 | tf_op jit(solution)/shard_map/ppermute | solution.py:258
  112.4 3.1 %collective-permute-start.1 = (bf16[512,256]{1,0:T(8,128)(2,1)S(1)}, bf16[512,256]{1,0:T(8,128)(2,1)S(1)}, u32[]{:S(2)}, u32[]{:S(2)}) collective-permute-start(bf16[512,256]{1,0:T(8,128)(2,1)S(1)} %constant_dynamic-update-slice_fusion.refs_1_.refs_3_), channel_id=1, source_target_pairs={{0,48},{16,0},{32,16},{48,32},{1,49},{17,1},{33,17},{49,33},{2,50}... | collective-permute-start | bytes 786440 | tf_op jit(solution)/shard_map/ppermute | solution.py:258
  118.1 4.2 %collective-permute-done.6.refs_2_ = bf16[256,128]{1,0:T(8,128)(2,1)S(1)} collective-permute-done((bf16[256,128]{1,0:T(8,128)(2,1)}, bf16[256,128]{1,0:T(8,128)(2,1)S(1)}, u32[]{:S(2)}, u32[]{:S(2)}) %collective-permute-start.6) | collective-permute-done | bytes 65568 | tf_op jit(solution)/shard_map/ppermute | solution.py:258
  123.6 2.3 %collective-permute-done.5.refs_1_ = bf16[256,128]{1,0:T(8,128)(2,1)S(1)} collective-permute-done((bf16[256,128]{1,0:T(8,128)(2,1)}, bf16[256,128]{1,0:T(8,128)(2,1)S(1)}, u32[]{:S(2)}, u32[]{:S(2)}) %collective-permute-start.5) | collective-permute-done | bytes 65568 | tf_op jit(solution)/shard_map/ppermute | solution.py:258
  125.9 4.5 %collective-permute-done.4.refs_0_ = bf16[256,128]{1,0:T(8,128)(2,1)S(1)} collective-permute-done((bf16[256,128]{1,0:T(8,128)(2,1)}, bf16[256,128]{1,0:T(8,128)(2,1)S(1)}, u32[]{:S(2)}, u32[]{:S(2)}) %collective-permute-start.4) | collective-permute-done | bytes 65568 | tf_op jit(solution)/shard_map/ppermute | solution.py:258
  132.0 6.7 %shard_map.178 = (bf16[264,256]{1,0:T(8,128)(2,1)}, bf16[264,256]{1,0:T(8,128)(2,1)}, bf16[264,256]{1,0:T(8,128)(2,1)}) custom-call(bf16[256,128]{1,0:T(8,128)(2,1)} %copy-done.17, bf16[256,128]{1,0:T(8,128)(2,1)} %copy-done.16, bf16[256,128]{1,0:T(8,128)(2,1)} %copy-done.15, bf16[512,256]{1,0:T(8,128)(2,1)} %copy-done.4, bf16[512,256]{1,0:T(8,128)(2,1)} %copy-done.7, ...), custom_call_target="tpu_custom_call" | custom-call | tf_op jit(solution)/shard_map/pallas_call | solution.py:324
  140.0 1.3 collective-permute-start.8
  141.3 1.3 collective-permute-start.9
  143.3 3.5 %shard_map.177.refs_0_ = bf16[264,256]{1,0:T(8,128)(2,1)} custom-call(bf16[256,128]{1,0:T(8,128)(2,1)} %get-tuple-element.9.refs_0_, bf16[512,256]{1,0:T(8,128)(2,1)} %copy-done.4, bf16[512,256]{1,0:T(8,128)(2,1)} %copy-done.7, bf16[512,256]{1,0:T(8,128)(2,1)} %copy-done.6, bf16[512,256]{1,0:T(8,128)(2,1)} %copy-done.5), custom_call_target="tpu_custom_call" | custom-call | tf_op jit(solution)/shard_map/pallas_call | solution.py:324
  147.6 2.4 %shard_map.179 = bf16[16,128,128]{2,1,0:T(8,128)(2,1)} custom-call(f32[1]{0:T(128)S(6)} %copy.22.lam_ref, bf16[264,256]{1,0:T(8,128)(2,1)} %shard_map.177.refs_0_, bf16[264,256]{1,0:T(8,128)(2,1)} %copy-done.12, bf16[264,256]{1,0:T(8,128)(2,1)} %copy-done.13, bf16[264,256]{1,0:T(8,128)(2,1)} %copy-done.14, f32[1,128]{1,0:T(1,128)} %bitcast.14), custom_call_target="tpu_custom_call" | custom-call | tf_op jit(solution)/shard_map/pallas_call | solution.py:345
  149.9 12.6 %all-to-all-start = ((bf16[16,128,128]{2,1,0:T(8,128)(2,1)}), bf16[16,128,128]{2,1,0:T(8,128)(2,1)S(1)}, u32[]{:S(2)}, u32[]{:S(2)}) async-start(bf16[16,128,128]{2,1,0:T(8,128)(2,1)} %shard_map.179), calls=%async_computation | async-start | bytes 1048576 | tf_op jit(solution)/shard_map/all_to_all | solution.py:249
  162.5 2.2 %collective-permute-start.10 = (bf16[2048,128]{1,0:T(8,128)(2,1)S(1)}, bf16[2048,128]{1,0:T(8,128)(2,1)S(1)}, u32[]{:S(2)}, u32[]{:S(2)}) collective-permute-start(bf16[2048,128]{1,0:T(8,128)(2,1)S(1)} %copy-done.9), channel_id=1, source_target_pairs={{0,1},{1,0},{2,3},{3,2},{4,5},{5,4},{6,7},{7,6},{8,9},{9,8},{10,11... | collective-permute-start | bytes 1572872 | tf_op jit(solution)/shard_map/ppermute | solution.py:253
  164.7 3.8 %shard_map.184 = bf16[32,4,8,128]{3,2,1,0:T(8,128)(2,1)} custom-call(bf16[4,4,192,128]{3,2,1,0:T(8,128)(2,1)} %copy-done.2, bf16[3,2048,128]{2,1,0:T(8,128)(2,1)} %copy-done, bf16[3,2048,128]{2,1,0:T(8,128)(2,1)} %collective-permute-done.12.refs_2_.refs_3_.refs_1_, bf16[3,2048,128]{2,1,0:T(8,128)(2,1)} %copy-done.1, ...), custom_call_target="tpu_custom_call" | custom-call | tf_op jit(solution)/shard_map/pallas_call | solution.py:335
  168.5 11.2 %all-to-all-done.rows_ref = bf16[16,128,128]{2,1,0:T(8,128)(2,1)S(1)} async-done(((bf16[16,128,128]{2,1,0:T(8,128)(2,1)}), bf16[16,128,128]{2,1,0:T(8,128)(2,1)S(1)}, u32[]{:S(2)}, u32[]{:S(2)}) %all-to-all-start) | async-done | bytes 524320 | tf_op jit(solution)/shard_map/all_to_all | solution.py:249
  179.7 7.1 %all-to-all-start.3 = ((bf16[128,8,128]{2,1,0:T(8,128)(2,1)}), bf16[128,8,128]{2,1,0:T(8,128)(2,1)S(1)}, u32[]{:S(2)}, u32[]{:S(2)}) async-start(bf16[128,8,128]{2,1,0:T(8,128)(2,1)} %bitcast.8), calls=%async_computation.3 | async-start | bytes 524288 | tf_op jit(solution)/shard_map/all_to_all | solution.py:249
  187.7 2.3 %shard_map.180 = (bf16[256,128]{1,0:T(8,128)(2,1)}, bf16[128,128]{1,0:T(8,128)(2,1)}) custom-call(bf16[16,128,128]{2,1,0:T(8,128)(2,1)} %copy-done.3, bf16[2048,128]{1,0:T(8,128)(2,1)} %own_ref.1, bf16[2048,128]{1,0:T(8,128)(2,1)} %copy-done.10), custom_call_target="tpu_custom_call" | custom-call | tf_op jit(solution)/shard_map/pallas_call | solution.py:349
  190.0 2.8 %collective-permute-start.11 = (bf16[128,128]{1,0:T(8,128)(2,1)}, bf16[128,128]{1,0:T(8,128)(2,1)S(1)}, u32[]{:S(2)}, u32[]{:S(2)}) collective-permute-start(bf16[128,128]{1,0:T(8,128)(2,1)} %get-tuple-element.15), channel_id=1, source_target_pairs={{0,1},{1,0},{2,3},{3,2},{4,5},{5,4},{6,7},{7,6},{8,9},{9,8},{10,11... | collective-permute-start | bytes 98312 | tf_op jit(solution)/shard_map/ppermute | solution.py:253
  194.4 1.5 shard_map.181
  195.9 4.6 %all-to-all-done.3.rows_ref = bf16[128,8,128]{2,1,0:T(8,128)(2,1)S(1)} async-done(((bf16[128,8,128]{2,1,0:T(8,128)(2,1)}), bf16[128,8,128]{2,1,0:T(8,128)(2,1)S(1)}, u32[]{:S(2)}, u32[]{:S(2)}) %all-to-all-start.3) | async-done | bytes 262176 | tf_op jit(solution)/shard_map/all_to_all | solution.py:249
  201.2 2.2 %shard_map.185 = bf16[128,128]{1,0:T(8,128)(2,1)} custom-call(s32[4,128]{1,0:T(4,128)} %bitcast.12, f32[4,128]{1,0:T(4,128)} %bitcast.13, bf16[128,8,128]{2,1,0:T(8,128)(2,1)} %copy-done.8), custom_call_target="tpu_custom_call" | custom-call | tf_op jit(solution)/shard_map/pallas_call | solution.py:360
  (58 shorter events, 14.0 us)
Async XLA Ops:
  0.6 2.3 %copy-start.11 = (bf16[1,2048,128]{2,1,0:T(8,128)(2,1)S(1)}, bf16[1,2048,128]{2,1,0:T(8,128)(2,1)}, u32[]{:S(2)}) copy-start(bf16[1,2048,128]{2,1,0:T(8,128)(2,1)} %param.33) | copy-start | bytes 1572868
  3.0 80.1 %copy-start = (bf16[3,2048,128]{2,1,0:T(8,128)(2,1)}, bf16[3,2048,128]{2,1,0:T(8,128)(2,1)S(1)}, u32[]{:S(2)}) copy-start(bf16[3,2048,128]{2,1,0:T(8,128)(2,1)S(1)} %constant_dynamic-update-slice_fusion.2.refs_0_.refs_1_) | copy-start | bytes 4718596
  3.0 33.3 %collective-permute-start.13 = (bf16[3,2048,128]{2,1,0:T(8,128)(2,1)S(1)}, bf16[3,2048,128]{2,1,0:T(8,128)(2,1)S(1)}, u32[]{:S(2)}, u32[]{:S(2)}) collective-permute-start(bf16[3,2048,128]{2,1,0:T(8,128)(2,1)S(1)} %constant_dynamic-update-slice_fusion.2.refs_0_.refs_1_), channel_id=1, source_target_pairs={{0,2},{2,0},{1,3},{3,1},{4,6},{6,4},{5,7},{7,5},{8,10},{10,8},{9,1... | collective-permute-start | bytes 4718600 | tf_op jit(solution)/shard_map/ppermute | solution.py:253
  7.0 76.0 %collective-permute-start.12 = (bf16[3,2048,128]{2,1,0:T(8,128)(2,1)S(1)}, bf16[3,2048,128]{2,1,0:T(8,128)(2,1)}, u32[]{:S(2)}, u32[]{:S(2)}) collective-permute-start(bf16[3,2048,128]{2,1,0:T(8,128)(2,1)S(1)} %constant_dynamic-update-slice_fusion.2.refs_0_.refs_1_), channel_id=1, source_target_pairs={{0,1},{1,0},{2,3},{3,2},{4,5},{5,4},{6,7},{7,6},{8,9},{9,8},{10,11... | collective-permute-start | bytes 4718600 | tf_op jit(solution)/shard_map/ppermute | solution.py:253
  36.3 46.7 %copy-start.1 = (bf16[3,2048,128]{2,1,0:T(8,128)(2,1)}, bf16[3,2048,128]{2,1,0:T(8,128)(2,1)S(1)}, u32[]{:S(2)}) copy-start(bf16[3,2048,128]{2,1,0:T(8,128)(2,1)S(1)} %collective-permute-done.13.refs_4_.refs_5_.refs_2_) | copy-start | bytes 4718596
  36.3 46.7 %collective-permute-start.14 = (bf16[3,2048,128]{2,1,0:T(8,128)(2,1)S(1)}, bf16[3,2048,128]{2,1,0:T(8,128)(2,1)}, u32[]{:S(2)}, u32[]{:S(2)}) collective-permute-start(bf16[3,2048,128]{2,1,0:T(8,128)(2,1)S(1)} %collective-permute-done.13.refs_4_.refs_5_.refs_2_), channel_id=1, source_target_pairs={{0,1},{1,0},{2,3},{3,2},{4,5},{5,4},{6,7},{7,6},{8,9},{9,8},{10,11... | collective-permute-start | bytes 4718600 | tf_op jit(solution)/shard_map/ppermute | solution.py:253
  88.0 62.0 %all-to-all-start.2 = ((bf16[4,4,192,128]{3,2,1,0:T(8,128)(2,1)}), bf16[4,4,192,128]{3,2,1,0:T(8,128)(2,1)S(1)}, u32[]{:S(2)}, u32[]{:S(2)}) async-start(bf16[4,4,192,128]{3,2,1,0:T(8,128)(2,1)} %shard_map.183), calls=%async_computation.2 | async-start | bytes 1572864 | tf_op jit(solution)/shard_map/all_to_all | solution.py:249
  98.3 6.2 %collective-permute-start = (bf16[256,256]{1,0:T(8,128)(2,1)}, bf16[256,256]{1,0:T(8,128)(2,1)S(1)}, u32[]{:S(2)}, u32[]{:S(2)}) collective-permute-start(bf16[256,256]{1,0:T(8,128)(2,1)} %get-tuple-element.10), channel_id=1, source_target_pairs={{0,64},{64,0},{1,65},{65,1},{2,66},{66,2},{3,67},{67,3},{4,68},{68... | collective-permute-start | bytes 393224 | tf_op jit(solution)/shard_map/ppermute | solution.py:253
  104.5 26.0 %copy-start.4 = (bf16[512,256]{1,0:T(8,128)(2,1)}, bf16[512,256]{1,0:T(8,128)(2,1)S(1)}, u32[]{:S(2)}) copy-start(bf16[512,256]{1,0:T(8,128)(2,1)S(1)} %constant_dynamic-update-slice_fusion.refs_1_.refs_3_) | copy-start | bytes 786436
  104.5 25.9 %collective-permute-start.3 = (bf16[512,256]{1,0:T(8,128)(2,1)S(1)}, bf16[512,256]{1,0:T(8,128)(2,1)S(1)}, u32[]{:S(2)}, u32[]{:S(2)}) collective-permute-start(bf16[512,256]{1,0:T(8,128)(2,1)S(1)} %constant_dynamic-update-slice_fusion.refs_1_.refs_3_), channel_id=1, source_target_pairs={{0,16},{16,32},{32,48},{48,0},{1,17},{17,33},{33,49},{49,1},{2,18}... | collective-permute-start | bytes 786440 | tf_op jit(solution)/shard_map/ppermute | solution.py:258
  107.4 23.1 %collective-permute-start.2 = (bf16[512,256]{1,0:T(8,128)(2,1)S(1)}, bf16[512,256]{1,0:T(8,128)(2,1)S(1)}, u32[]{:S(2)}, u32[]{:S(2)}) collective-permute-start(bf16[512,256]{1,0:T(8,128)(2,1)S(1)} %constant_dynamic-update-slice_fusion.refs_1_.refs_3_), channel_id=1, source_target_pairs={{0,32},{16,48},{32,0},{48,16},{1,33},{17,49},{33,1},{49,17},{2,34}... | collective-permute-start | bytes 786440 | tf_op jit(solution)/shard_map/ppermute | solution.py:258
  112.4 18.0 %collective-permute-start.1 = (bf16[512,256]{1,0:T(8,128)(2,1)S(1)}, bf16[512,256]{1,0:T(8,128)(2,1)S(1)}, u32[]{:S(2)}, u32[]{:S(2)}) collective-permute-start(bf16[512,256]{1,0:T(8,128)(2,1)S(1)} %constant_dynamic-update-slice_fusion.refs_1_.refs_3_), channel_id=1, source_target_pairs={{0,48},{16,0},{32,16},{48,32},{1,49},{17,1},{33,17},{49,33},{2,50}... | collective-permute-start | bytes 786440 | tf_op jit(solution)/shard_map/ppermute | solution.py:258
  115.5 6.8 %collective-permute-start.6 = (bf16[256,128]{1,0:T(8,128)(2,1)}, bf16[256,128]{1,0:T(8,128)(2,1)S(1)}, u32[]{:S(2)}, u32[]{:S(2)}) collective-permute-start(bf16[256,128]{1,0:T(8,128)(2,1)} %get-tuple-element.9.refs_0_), channel_id=1, source_target_pairs={{128,0},{256,128},{384,256},{129,1},{257,129},{385,257},{130,2},{2... | collective-permute-start | bytes 196616 | tf_op jit(solution)/shard_map/ppermute | solution.py:258
  116.8 9.1 %collective-permute-start.5 = (bf16[256,128]{1,0:T(8,128)(2,1)}, bf16[256,128]{1,0:T(8,128)(2,1)S(1)}, u32[]{:S(2)}, u32[]{:S(2)}) collective-permute-start(bf16[256,128]{1,0:T(8,128)(2,1)} %get-tuple-element.9.refs_0_), channel_id=1, source_target_pairs={{256,0},{384,128},{257,1},{385,129},{258,2},{386,130},{259,3},{387... | collective-permute-start | bytes 196616 | tf_op jit(solution)/shard_map/ppermute | solution.py:258
  122.3 8.1 %copy-start.15 = (bf16[256,128]{1,0:T(8,128)(2,1)}, bf16[256,128]{1,0:T(8,128)(2,1)S(1)}, u32[]{:S(2)}) copy-start(bf16[256,128]{1,0:T(8,128)(2,1)S(1)} %collective-permute-done.6.refs_2_) | copy-start | bytes 196612
  122.4 8.1 %collective-permute-start.4 = (bf16[256,128]{1,0:T(8,128)(2,1)}, bf16[256,128]{1,0:T(8,128)(2,1)S(1)}, u32[]{:S(2)}, u32[]{:S(2)}) collective-permute-start(bf16[256,128]{1,0:T(8,128)(2,1)} %get-tuple-element.9.refs_0_), channel_id=1, source_target_pairs={{384,0},{385,1},{386,2},{387,3},{388,4},{389,5},{390,6},{391,7},{3... | collective-permute-start | bytes 196616 | tf_op jit(solution)/shard_map/ppermute | solution.py:258
  125.9 4.6 %copy-start.16 = (bf16[256,128]{1,0:T(8,128)(2,1)}, bf16[256,128]{1,0:T(8,128)(2,1)S(1)}, u32[]{:S(2)}) copy-start(bf16[256,128]{1,0:T(8,128)(2,1)S(1)} %collective-permute-done.5.refs_1_) | copy-start | bytes 196612
  130.4 0.8 copy-start.5
  130.4 0.9 copy-start.6
  138.8 8.0 %collective-permute-start.7 = (bf16[264,256]{1,0:T(8,128)(2,1)}, bf16[264,256]{1,0:T(8,128)(2,1)S(1)}, u32[]{:S(2)}, u32[]{:S(2)}) collective-permute-start(bf16[264,256]{1,0:T(8,128)(2,1)} %get-tuple-element.11), channel_id=1, source_target_pairs={{0,128},{128,256},{256,384},{1,129},{129,257},{257,385},{2,130},{1... | collective-permute-start | bytes 405512 | tf_op jit(solution)/shard_map/ppermute | solution.py:258
  140.0 6.7 %collective-permute-start.8 = (bf16[264,256]{1,0:T(8,128)(2,1)}, bf16[264,256]{1,0:T(8,128)(2,1)S(1)}, u32[]{:S(2)}, u32[]{:S(2)}) collective-permute-start(bf16[264,256]{1,0:T(8,128)(2,1)} %get-tuple-element.12), channel_id=1, source_target_pairs={{0,256},{128,384},{1,257},{129,385},{2,258},{130,386},{3,259},{131... | collective-permute-start | bytes 405512 | tf_op jit(solution)/shard_map/ppermute | solution.py:258
  141.3 5.5 %collective-permute-start.9 = (bf16[264,256]{1,0:T(8,128)(2,1)}, bf16[264,256]{1,0:T(8,128)(2,1)S(1)}, u32[]{:S(2)}, u32[]{:S(2)}) collective-permute-start(bf16[264,256]{1,0:T(8,128)(2,1)} %get-tuple-element.13), channel_id=1, source_target_pairs={{0,384},{1,385},{2,386},{3,387},{4,388},{5,389},{6,390},{7,391},{8... | collective-permute-start | bytes 405512 | tf_op jit(solution)/shard_map/ppermute | solution.py:258
  143.3 19.2 %copy-start.9 = (bf16[2048,128]{1,0:T(8,128)(2,1)S(1)}, bf16[2048,128]{1,0:T(8,128)(2,1)}, u32[]{:S(2)}) copy-start(bf16[2048,128]{1,0:T(8,128)(2,1)} %own_ref.1) | copy-start | bytes 1572868
  146.8 0.7 copy-start.13
  146.8 0.7 copy-start.14
  149.9 14.8 %copy-start.2 = (bf16[4,4,192,128]{3,2,1,0:T(8,128)(2,1)}, bf16[4,4,192,128]{3,2,1,0:T(8,128)(2,1)S(1)}, u32[]{:S(2)}) copy-start(bf16[4,4,192,128]{3,2,1,0:T(8,128)(2,1)S(1)} %all-to-all-done.2.hidden_ref) | copy-start | bytes 2359300
  149.9 29.8 %all-to-all-start = ((bf16[16,128,128]{2,1,0:T(8,128)(2,1)}), bf16[16,128,128]{2,1,0:T(8,128)(2,1)S(1)}, u32[]{:S(2)}, u32[]{:S(2)}) async-start(bf16[16,128,128]{2,1,0:T(8,128)(2,1)} %shard_map.179), calls=%async_computation | async-start | bytes 1048576 | tf_op jit(solution)/shard_map/all_to_all | solution.py:249
  162.5 24.3 %collective-permute-start.10 = (bf16[2048,128]{1,0:T(8,128)(2,1)S(1)}, bf16[2048,128]{1,0:T(8,128)(2,1)S(1)}, u32[]{:S(2)}, u32[]{:S(2)}) collective-permute-start(bf16[2048,128]{1,0:T(8,128)(2,1)S(1)} %copy-done.9), channel_id=1, source_target_pairs={{0,1},{1,0},{2,3},{3,2},{4,5},{5,4},{6,7},{7,6},{8,9},{9,8},{10,11... | collective-permute-start | bytes 1572872 | tf_op jit(solution)/shard_map/ppermute | solution.py:253
  179.7 7.1 %copy-start.3 = (bf16[16,128,128]{2,1,0:T(8,128)(2,1)}, bf16[16,128,128]{2,1,0:T(8,128)(2,1)S(1)}, u32[]{:S(2)}) copy-start(bf16[16,128,128]{2,1,0:T(8,128)(2,1)S(1)} %all-to-all-done.rows_ref) | copy-start | bytes 1572868
  179.7 20.8 %all-to-all-start.3 = ((bf16[128,8,128]{2,1,0:T(8,128)(2,1)}), bf16[128,8,128]{2,1,0:T(8,128)(2,1)S(1)}, u32[]{:S(2)}, u32[]{:S(2)}) async-start(bf16[128,8,128]{2,1,0:T(8,128)(2,1)} %bitcast.8), calls=%async_computation.3 | async-start | bytes 524288 | tf_op jit(solution)/shard_map/all_to_all | solution.py:249
  186.8 0.8 copy-start.10
  190.0 3.8 %collective-permute-start.11 = (bf16[128,128]{1,0:T(8,128)(2,1)}, bf16[128,128]{1,0:T(8,128)(2,1)S(1)}, u32[]{:S(2)}, u32[]{:S(2)}) collective-permute-start(bf16[128,128]{1,0:T(8,128)(2,1)} %get-tuple-element.15), channel_id=1, source_target_pairs={{0,1},{1,0},{2,3},{3,2},{4,5},{5,4},{6,7},{7,6},{8,9},{9,8},{10,11... | collective-permute-start | bytes 98312 | tf_op jit(solution)/shard_map/ppermute | solution.py:253
  (5 other events, 3.3 us)

commit v4 on v3

--- a/solution.py
+++ b/solution.py
@@ -72,11 +72,11 @@
     wanted = (row % 6 + 6 * corner()).astype(F32)
     hit = wide == wanted
     normed = rms(x_ref[...].astype(F32), gain_ref[...], 1e-05).astype(BF)
-    total = None
-    for part in range(4):
-        pick = jnp.where(hit & (row // 6 == part), 1.0, 0.0).astype(BF)
-        piece = dot(pick, normed[:, part * chunk : (part + 1) * chunk])
-        total = piece if total is None else total + piece
+    picks = [
+        jnp.where(hit & (row // 6 == part), 1.0, 0.0).astype(BF) for part in range(4)
+    ]
+    pieces = [normed[:, part * chunk : (part + 1) * chunk] for part in range(4)]
+    total = dot(jnp.concatenate(picks, axis=1), jnp.concatenate(pieces, axis=0))
     out_ref[...] = total.astype(BF).reshape(out_ref.shape)
 
 

time: 204 us -> 204 us (level)
  no operation moved by 1% of the time
where the time goes in v4:
time: 204 us; the launch traced here: 203 us
  starting transfers between devices  70.7 us (35%)
  waiting for transfers between devices  53.8 us (26%)
  blocking collectives  35.2 us (17%)
  Pallas kernels  33.9 us (17%)
  local copies, waits for them, and re-layouts  7.7 us (4%)
    all_to_all x1, blocking collectives, exchange(): return lax.all_to_all(a, axes, 0, 0, tiled=True)  35.2 us
    ppermute x6, waiting for transfers between devices, swap(): return lax.ppermute(a, axes, [(n, n ^ flip) for n in range(size)])  27 us
    all_to_all x3, starting transfers between devices, exchange(): return lax.all_to_all(a, axes, 0, 0, tiled=True)  26.5 us
    ppermute x6, starting transfers between devices, swap(): return lax.ppermute(a, axes, [(n, n ^ flip) for n in range(size)])  25.5 us
    ppermute x9, starting transfers between devices, shift(): return lax.ppermute(a, axis, pairs)  18.7 us
    all_to_all x3, waiting for transfers between devices, exchange(): return lax.all_to_all(a, axes, 0, 0, tiled=True)  15.7 us
    ppermute x9, waiting for transfers between devices, shift(): return lax.ppermute(a, axis, pairs)  11.1 us
    pallas_call x2, Pallas kernels, body(): call(partial_kernel(steps), [shape((rows_a + 8, 256), BF)] * len(steps),...  10.2 us
  transfers between devices with their start and end apart: 18, of which 8 were waited for; matrix products, arithmetic and copies ran while one was open for 0% of the time, Pallas kernels for 13%

profile of v4, /device:TPU:1, one launch (start us, length us, event | category | flops | bytes accessed | tf_op | source)
XLA Modules:
  0.0 203.0 jit_solution(10163152608249927342)
XLA Ops:
  3.0 4.0 %collective-permute-start.13 = (bf16[3,2048,128]{2,1,0:T(8,128)(2,1)S(1)}, bf16[3,2048,128]{2,1,0:T(8,128)(2,1)S(1)}, u32[]{:S(2)}, u32[]{:S(2)}) collective-permute-start(bf16[3,2048,128]{2,1,0:T(8,128)(2,1)S(1)} %constant_dynamic-update-slice_fusion.2.refs_0_.refs_1_), channel_id=1, source_target_pairs={{0,2},{2,0},{1,3},{3,1},{4,6},{6,4},{5,7},{7,5},{8,10},{10,8},{9,1... | collective-permute-start | bytes 4718600 | tf_op jit(solution)/shard_map/ppermute | solution.py:253
  7.0 6.6 %collective-permute-start.12 = (bf16[3,2048,128]{2,1,0:T(8,128)(2,1)S(1)}, bf16[3,2048,128]{2,1,0:T(8,128)(2,1)}, u32[]{:S(2)}, u32[]{:S(2)}) collective-permute-start(bf16[3,2048,128]{2,1,0:T(8,128)(2,1)S(1)} %constant_dynamic-update-slice_fusion.2.refs_0_.refs_1_), channel_id=1, source_target_pairs={{0,1},{1,0},{2,3},{3,2},{4,5},{5,4},{6,7},{7,6},{8,9},{9,8},{10,11... | collective-permute-start | bytes 4718600 | tf_op jit(solution)/shard_map/ppermute | solution.py:253
  13.7 22.6 %collective-permute-done.13.refs_4_.refs_5_.refs_2_ = bf16[3,2048,128]{2,1,0:T(8,128)(2,1)S(1)} collective-permute-done((bf16[3,2048,128]{2,1,0:T(8,128)(2,1)S(1)}, bf16[3,2048,128]{2,1,0:T(8,128)(2,1)S(1)}, u32[]{:S(2)}, u32[]{:S(2)}) %collective-permute-start.13) | collective-permute-done | bytes 1572896 | tf_op jit(solution)/shard_map/ppermute | solution.py:253
  36.3 8.0 %collective-permute-start.14 = (bf16[3,2048,128]{2,1,0:T(8,128)(2,1)S(1)}, bf16[3,2048,128]{2,1,0:T(8,128)(2,1)}, u32[]{:S(2)}, u32[]{:S(2)}) collective-permute-start(bf16[3,2048,128]{2,1,0:T(8,128)(2,1)S(1)} %collective-permute-done.13.refs_4_.refs_5_.refs_2_), channel_id=1, source_target_pairs={{0,1},{1,0},{2,3},{3,2},{4,5},{5,4},{6,7},{7,6},{8,9},{9,8},{10,11... | collective-permute-start | bytes 4718600 | tf_op jit(solution)/shard_map/ppermute | solution.py:253
  44.3 3.2 %shard_map.182 = bf16[32,24,512]{2,1,0:T(8,128)(2,1)} custom-call(bf16[128,2048]{1,0:T(8,128)(2,1)} %x_ref.3, f32[1,2048]{1,0:T(1,128)} %bitcast.9, s32[4,128]{1,0:T(4,128)} %bitcast.11), custom_call_target="tpu_custom_call" | custom-call | tf_op jit(solution)/shard_map/pallas_call | solution.py:288
  47.4 35.2 %all_to_all.20.in_ref = bf16[32,24,512]{2,1,0:T(8,128)(2,1)} all-to-all(bf16[32,24,512]{2,1,0:T(8,128)(2,1)} %shard_map.182), channel_id=1, replica_groups=mesh['w'=4,'v'=2,'x'=4,'g'=4,'r'=2,'c'=2] {'w','v','x'}, dimensions={0} | all-to-all | bytes 1572864 | tf_op jit(solution)/shard_map/all_to_all | solution.py:249
  82.7 4.9 %shard_map.183 = bf16[4,4,192,128]{3,2,1,0:T(8,128)(2,1)} custom-call(bf16[32,24,512]{2,1,0:T(8,128)(2,1)} %all_to_all.20.in_ref, bf16[3,2048,128]{2,1,0:T(8,128)(2,1)} %copy-done, bf16[3,2048,128]{2,1,0:T(8,128)(2,1)} %copy-done, bf16[3,2048,128]{2,1,0:T(8,128)(2,1)} %collective-permute-done.12.refs_2_.refs_3_.refs_1_, ...), custom_call_target="tpu_custom_call" | custom-call | tf_op jit(solution)/shard_map/pallas_call | solution.py:313
  87.6 6.8 %all-to-all-start.2 = ((bf16[4,4,192,128]{3,2,1,0:T(8,128)(2,1)}), bf16[4,4,192,128]{3,2,1,0:T(8,128)(2,1)S(1)}, u32[]{:S(2)}, u32[]{:S(2)}) async-start(bf16[4,4,192,128]{3,2,1,0:T(8,128)(2,1)} %shard_map.183), calls=%async_computation.2 | async-start | bytes 1572864 | tf_op jit(solution)/shard_map/all_to_all | solution.py:249
  94.4 3.5 %shard_map.176 = (bf16[256,128]{1,0:T(8,128)(2,1)}, bf16[256,256]{1,0:T(8,128)(2,1)}) custom-call(bf16[256,2048]{1,0:T(8,128)(2,1)} %x_ref.2, f32[1,2048]{1,0:T(1,128)} %bitcast.10, bf16[2048,128]{1,0:T(8,128)(2,1)} %wq_ref.1, bf16[2048,128]{1,0:T(8,128)(2,1)} %wk_ref.1, bf16[2048,128]{1,0:T(8,128)(2,1)} %wv_ref.1, f32[1,64]{1,0:T(1,128)} %bitcast.15, ...), custom_call_target="tpu_custom_call" | custom-call | tf_op jit(solution)/shard_map/pallas_call | solution.py:293
  97.9 1.9 collective-permute-start
  100.8 3.4 %collective-permute-done = bf16[256,256]{1,0:T(8,128)(2,1)S(1)} collective-permute-done((bf16[256,256]{1,0:T(8,128)(2,1)}, bf16[256,256]{1,0:T(8,128)(2,1)S(1)}, u32[]{:S(2)}, u32[]{:S(2)}) %collective-permute-start) | collective-permute-done | bytes 131104 | tf_op jit(solution)/shard_map/ppermute | solution.py:253
  104.1 2.8 %collective-permute-start.3 = (bf16[512,256]{1,0:T(8,128)(2,1)S(1)}, bf16[512,256]{1,0:T(8,128)(2,1)S(1)}, u32[]{:S(2)}, u32[]{:S(2)}) collective-permute-start(bf16[512,256]{1,0:T(8,128)(2,1)S(1)} %constant_dynamic-update-slice_fusion.refs_1_.refs_3_), channel_id=1, source_target_pairs={{0,16},{16,32},{32,48},{48,0},{1,17},{17,33},{33,49},{49,1},{2,18}... | collective-permute-start | bytes 786440 | tf_op jit(solution)/shard_map/ppermute | solution.py:258
  107.0 5.1 %collective-permute-start.2 = (bf16[512,256]{1,0:T(8,128)(2,1)S(1)}, bf16[512,256]{1,0:T(8,128)(2,1)S(1)}, u32[]{:S(2)}, u32[]{:S(2)}) collective-permute-start(bf16[512,256]{1,0:T(8,128)(2,1)S(1)} %constant_dynamic-update-slice_fusion.refs_1_.refs_3_), channel_id=1, source_target_pairs={{0,32},{16,48},{32,0},{48,16},{1,33},{17,49},{33,1},{49,17},{2,34}... | collective-permute-start | bytes 786440 | tf_op jit(solution)/shard_map/ppermute | solution.py:258
  112.1 3.1 %collective-permute-start.1 = (bf16[512,256]{1,0:T(8,128)(2,1)S(1)}, bf16[512,256]{1,0:T(8,128)(2,1)S(1)}, u32[]{:S(2)}, u32[]{:S(2)}) collective-permute-start(bf16[512,256]{1,0:T(8,128)(2,1)S(1)} %constant_dynamic-update-slice_fusion.refs_1_.refs_3_), channel_id=1, source_target_pairs={{0,48},{16,0},{32,16},{48,32},{1,49},{17,1},{33,17},{49,33},{2,50}... | collective-permute-start | bytes 786440 | tf_op jit(solution)/shard_map/ppermute | solution.py:258
  117.8 4.2 %collective-permute-done.6.refs_2_ = bf16[256,128]{1,0:T(8,128)(2,1)S(1)} collective-permute-done((bf16[256,128]{1,0:T(8,128)(2,1)}, bf16[256,128]{1,0:T(8,128)(2,1)S(1)}, u32[]{:S(2)}, u32[]{:S(2)}) %collective-permute-start.6) | collective-permute-done | bytes 65568 | tf_op jit(solution)/shard_map/ppermute | solution.py:258
  123.3 2.3 %collective-permute-done.5.refs_1_ = bf16[256,128]{1,0:T(8,128)(2,1)S(1)} collective-permute-done((bf16[256,128]{1,0:T(8,128)(2,1)}, bf16[256,128]{1,0:T(8,128)(2,1)S(1)}, u32[]{:S(2)}, u32[]{:S(2)}) %collective-permute-start.5) | collective-permute-done | bytes 65568 | tf_op jit(solution)/shard_map/ppermute | solution.py:258
  125.6 4.5 %collective-permute-done.4.refs_0_ = bf16[256,128]{1,0:T(8,128)(2,1)S(1)} collective-permute-done((bf16[256,128]{1,0:T(8,128)(2,1)}, bf16[256,128]{1,0:T(8,128)(2,1)S(1)}, u32[]{:S(2)}, u32[]{:S(2)}) %collective-permute-start.4) | collective-permute-done | bytes 65568 | tf_op jit(solution)/shard_map/ppermute | solution.py:258
  131.7 6.7 %shard_map.178 = (bf16[264,256]{1,0:T(8,128)(2,1)}, bf16[264,256]{1,0:T(8,128)(2,1)}, bf16[264,256]{1,0:T(8,128)(2,1)}) custom-call(bf16[256,128]{1,0:T(8,128)(2,1)} %copy-done.17, bf16[256,128]{1,0:T(8,128)(2,1)} %copy-done.16, bf16[256,128]{1,0:T(8,128)(2,1)} %copy-done.15, bf16[512,256]{1,0:T(8,128)(2,1)} %copy-done.4, bf16[512,256]{1,0:T(8,128)(2,1)} %copy-done.7, ...), custom_call_target="tpu_custom_call" | custom-call | tf_op jit(solution)/shard_map/pallas_call | solution.py:324
  139.7 1.3 collective-permute-start.8
  141.0 1.3 collective-permute-start.9
  143.0 3.5 %shard_map.177.refs_0_ = bf16[264,256]{1,0:T(8,128)(2,1)} custom-call(bf16[256,128]{1,0:T(8,128)(2,1)} %get-tuple-element.9.refs_0_, bf16[512,256]{1,0:T(8,128)(2,1)} %copy-done.4, bf16[512,256]{1,0:T(8,128)(2,1)} %copy-done.7, bf16[512,256]{1,0:T(8,128)(2,1)} %copy-done.6, bf16[512,256]{1,0:T(8,128)(2,1)} %copy-done.5), custom_call_target="tpu_custom_call" | custom-call | tf_op jit(solution)/shard_map/pallas_call | solution.py:324
  147.2 2.4 %shard_map.179 = bf16[16,128,128]{2,1,0:T(8,128)(2,1)} custom-call(f32[1]{0:T(128)S(6)} %copy.22.lam_ref, bf16[264,256]{1,0:T(8,128)(2,1)} %shard_map.177.refs_0_, bf16[264,256]{1,0:T(8,128)(2,1)} %copy-done.12, bf16[264,256]{1,0:T(8,128)(2,1)} %copy-done.13, bf16[264,256]{1,0:T(8,128)(2,1)} %copy-done.14, f32[1,128]{1,0:T(1,128)} %bitcast.14), custom_call_target="tpu_custom_call" | custom-call | tf_op jit(solution)/shard_map/pallas_call | solution.py:345
  149.6 12.6 %all-to-all-start = ((bf16[16,128,128]{2,1,0:T(8,128)(2,1)}), bf16[16,128,128]{2,1,0:T(8,128)(2,1)S(1)}, u32[]{:S(2)}, u32[]{:S(2)}) async-start(bf16[16,128,128]{2,1,0:T(8,128)(2,1)} %shard_map.179), calls=%async_computation | async-start | bytes 1048576 | tf_op jit(solution)/shard_map/all_to_all | solution.py:249
  162.1 2.2 %collective-permute-start.10 = (bf16[2048,128]{1,0:T(8,128)(2,1)S(1)}, bf16[2048,128]{1,0:T(8,128)(2,1)S(1)}, u32[]{:S(2)}, u32[]{:S(2)}) collective-permute-start(bf16[2048,128]{1,0:T(8,128)(2,1)S(1)} %copy-done.9), channel_id=1, source_target_pairs={{0,1},{1,0},{2,3},{3,2},{4,5},{5,4},{6,7},{7,6},{8,9},{9,8},{10,11... | collective-permute-start | bytes 1572872 | tf_op jit(solution)/shard_map/ppermute | solution.py:253
  164.3 3.8 %shard_map.184 = bf16[32,4,8,128]{3,2,1,0:T(8,128)(2,1)} custom-call(bf16[4,4,192,128]{3,2,1,0:T(8,128)(2,1)} %copy-done.2, bf16[3,2048,128]{2,1,0:T(8,128)(2,1)} %copy-done, bf16[3,2048,128]{2,1,0:T(8,128)(2,1)} %collective-permute-done.12.refs_2_.refs_3_.refs_1_, bf16[3,2048,128]{2,1,0:T(8,128)(2,1)} %copy-done.1, ...), custom_call_target="tpu_custom_call" | custom-call | tf_op jit(solution)/shard_map/pallas_call | solution.py:335
  168.2 11.2 %all-to-all-done.rows_ref = bf16[16,128,128]{2,1,0:T(8,128)(2,1)S(1)} async-done(((bf16[16,128,128]{2,1,0:T(8,128)(2,1)}), bf16[16,128,128]{2,1,0:T(8,128)(2,1)S(1)}, u32[]{:S(2)}, u32[]{:S(2)}) %all-to-all-start) | async-done | bytes 524320 | tf_op jit(solution)/shard_map/all_to_all | solution.py:249
  179.3 7.1 %all-to-all-start.3 = ((bf16[128,8,128]{2,1,0:T(8,128)(2,1)}), bf16[128,8,128]{2,1,0:T(8,128)(2,1)S(1)}, u32[]{:S(2)}, u32[]{:S(2)}) async-start(bf16[128,8,128]{2,1,0:T(8,128)(2,1)} %bitcast.8), calls=%async_computation.3 | async-start | bytes 524288 | tf_op jit(solution)/shard_map/all_to_all | solution.py:249
  187.3 2.3 %shard_map.180 = (bf16[256,128]{1,0:T(8,128)(2,1)}, bf16[128,128]{1,0:T(8,128)(2,1)}) custom-call(bf16[16,128,128]{2,1,0:T(8,128)(2,1)} %copy-done.3, bf16[2048,128]{1,0:T(8,128)(2,1)} %own_ref.1, bf16[2048,128]{1,0:T(8,128)(2,1)} %copy-done.10), custom_call_target="tpu_custom_call" | custom-call | tf_op jit(solution)/shard_map/pallas_call | solution.py:349
  189.6 2.8 %collective-permute-start.11 = (bf16[128,128]{1,0:T(8,128)(2,1)}, bf16[128,128]{1,0:T(8,128)(2,1)S(1)}, u32[]{:S(2)}, u32[]{:S(2)}) collective-permute-start(bf16[128,128]{1,0:T(8,128)(2,1)} %get-tuple-element.15), channel_id=1, source_target_pairs={{0,1},{1,0},{2,3},{3,2},{4,5},{5,4},{6,7},{7,6},{8,9},{9,8},{10,11... | collective-permute-start | bytes 98312 | tf_op jit(solution)/shard_map/ppermute | solution.py:253
  194.1 1.5 shard_map.181
  195.6 4.6 %all-to-all-done.3.rows_ref = bf16[128,8,128]{2,1,0:T(8,128)(2,1)S(1)} async-done(((bf16[128,8,128]{2,1,0:T(8,128)(2,1)}), bf16[128,8,128]{2,1,0:T(8,128)(2,1)S(1)}, u32[]{:S(2)}, u32[]{:S(2)}) %all-to-all-start.3) | async-done | bytes 262176 | tf_op jit(solution)/shard_map/all_to_all | solution.py:249
  200.8 2.2 %shard_map.185 = bf16[128,128]{1,0:T(8,128)(2,1)} custom-call(s32[4,128]{1,0:T(4,128)} %bitcast.12, f32[4,128]{1,0:T(4,128)} %bitcast.13, bf16[128,8,128]{2,1,0:T(8,128)(2,1)} %copy-done.8), custom_call_target="tpu_custom_call" | custom-call | tf_op jit(solution)/shard_map/pallas_call | solution.py:360
  (58 shorter events, 14.0 us)
Async XLA Ops:
  0.6 2.3 %copy-start.11 = (bf16[1,2048,128]{2,1,0:T(8,128)(2,1)S(1)}, bf16[1,2048,128]{2,1,0:T(8,128)(2,1)}, u32[]{:S(2)}) copy-start(bf16[1,2048,128]{2,1,0:T(8,128)(2,1)} %param.33) | copy-start | bytes 1572868
  3.0 79.7 %copy-start = (bf16[3,2048,128]{2,1,0:T(8,128)(2,1)}, bf16[3,2048,128]{2,1,0:T(8,128)(2,1)S(1)}, u32[]{:S(2)}) copy-start(bf16[3,2048,128]{2,1,0:T(8,128)(2,1)S(1)} %constant_dynamic-update-slice_fusion.2.refs_0_.refs_1_) | copy-start | bytes 4718596
  3.0 33.3 %collective-permute-start.13 = (bf16[3,2048,128]{2,1,0:T(8,128)(2,1)S(1)}, bf16[3,2048,128]{2,1,0:T(8,128)(2,1)S(1)}, u32[]{:S(2)}, u32[]{:S(2)}) collective-permute-start(bf16[3,2048,128]{2,1,0:T(8,128)(2,1)S(1)} %constant_dynamic-update-slice_fusion.2.refs_0_.refs_1_), channel_id=1, source_target_pairs={{0,2},{2,0},{1,3},{3,1},{4,6},{6,4},{5,7},{7,5},{8,10},{10,8},{9,1... | collective-permute-start | bytes 4718600 | tf_op jit(solution)/shard_map/ppermute | solution.py:253
  7.0 75.7 %collective-permute-start.12 = (bf16[3,2048,128]{2,1,0:T(8,128)(2,1)S(1)}, bf16[3,2048,128]{2,1,0:T(8,128)(2,1)}, u32[]{:S(2)}, u32[]{:S(2)}) collective-permute-start(bf16[3,2048,128]{2,1,0:T(8,128)(2,1)S(1)} %constant_dynamic-update-slice_fusion.2.refs_0_.refs_1_), channel_id=1, source_target_pairs={{0,1},{1,0},{2,3},{3,2},{4,5},{5,4},{6,7},{7,6},{8,9},{9,8},{10,11... | collective-permute-start | bytes 4718600 | tf_op jit(solution)/shard_map/ppermute | solution.py:253
  36.3 46.4 %copy-start.1 = (bf16[3,2048,128]{2,1,0:T(8,128)(2,1)}, bf16[3,2048,128]{2,1,0:T(8,128)(2,1)S(1)}, u32[]{:S(2)}) copy-start(bf16[3,2048,128]{2,1,0:T(8,128)(2,1)S(1)} %collective-permute-done.13.refs_4_.refs_5_.refs_2_) | copy-start | bytes 4718596
  36.3 46.4 %collective-permute-start.14 = (bf16[3,2048,128]{2,1,0:T(8,128)(2,1)S(1)}, bf16[3,2048,128]{2,1,0:T(8,128)(2,1)}, u32[]{:S(2)}, u32[]{:S(2)}) collective-permute-start(bf16[3,2048,128]{2,1,0:T(8,128)(2,1)S(1)} %collective-permute-done.13.refs_4_.refs_5_.refs_2_), channel_id=1, source_target_pairs={{0,1},{1,0},{2,3},{3,2},{4,5},{5,4},{6,7},{7,6},{8,9},{9,8},{10,11... | collective-permute-start | bytes 4718600 | tf_op jit(solution)/shard_map/ppermute | solution.py:253
  87.6 62.0 %all-to-all-start.2 = ((bf16[4,4,192,128]{3,2,1,0:T(8,128)(2,1)}), bf16[4,4,192,128]{3,2,1,0:T(8,128)(2,1)S(1)}, u32[]{:S(2)}, u32[]{:S(2)}) async-start(bf16[4,4,192,128]{3,2,1,0:T(8,128)(2,1)} %shard_map.183), calls=%async_computation.2 | async-start | bytes 1572864 | tf_op jit(solution)/shard_map/all_to_all | solution.py:249
  97.9 6.2 %collective-permute-start = (bf16[256,256]{1,0:T(8,128)(2,1)}, bf16[256,256]{1,0:T(8,128)(2,1)S(1)}, u32[]{:S(2)}, u32[]{:S(2)}) collective-permute-start(bf16[256,256]{1,0:T(8,128)(2,1)} %get-tuple-element.10), channel_id=1, source_target_pairs={{0,64},{64,0},{1,65},{65,1},{2,66},{66,2},{3,67},{67,3},{4,68},{68... | collective-permute-start | bytes 393224 | tf_op jit(solution)/shard_map/ppermute | solution.py:253
  104.1 26.0 %copy-start.4 = (bf16[512,256]{1,0:T(8,128)(2,1)}, bf16[512,256]{1,0:T(8,128)(2,1)S(1)}, u32[]{:S(2)}) copy-start(bf16[512,256]{1,0:T(8,128)(2,1)S(1)} %constant_dynamic-update-slice_fusion.refs_1_.refs_3_) | copy-start | bytes 786436
  104.1 25.9 %collective-permute-start.3 = (bf16[512,256]{1,0:T(8,128)(2,1)S(1)}, bf16[512,256]{1,0:T(8,128)(2,1)S(1)}, u32[]{:S(2)}, u32[]{:S(2)}) collective-permute-start(bf16[512,256]{1,0:T(8,128)(2,1)S(1)} %constant_dynamic-update-slice_fusion.refs_1_.refs_3_), channel_id=1, source_target_pairs={{0,16},{16,32},{32,48},{48,0},{1,17},{17,33},{33,49},{49,1},{2,18}... | collective-permute-start | bytes 786440 | tf_op jit(solution)/shard_map/ppermute | solution.py:258
  107.0 23.1 %collective-permute-start.2 = (bf16[512,256]{1,0:T(8,128)(2,1)S(1)}, bf16[512,256]{1,0:T(8,128)(2,1)S(1)}, u32[]{:S(2)}, u32[]{:S(2)}) collective-permute-start(bf16[512,256]{1,0:T(8,128)(2,1)S(1)} %constant_dynamic-update-slice_fusion.refs_1_.refs_3_), channel_id=1, source_target_pairs={{0,32},{16,48},{32,0},{48,16},{1,33},{17,49},{33,1},{49,17},{2,34}... | collective-permute-start | bytes 786440 | tf_op jit(solution)/shard_map/ppermute | solution.py:258
  112.1 18.0 %collective-permute-start.1 = (bf16[512,256]{1,0:T(8,128)(2,1)S(1)}, bf16[512,256]{1,0:T(8,128)(2,1)S(1)}, u32[]{:S(2)}, u32[]{:S(2)}) collective-permute-start(bf16[512,256]{1,0:T(8,128)(2,1)S(1)} %constant_dynamic-update-slice_fusion.refs_1_.refs_3_), channel_id=1, source_target_pairs={{0,48},{16,0},{32,16},{48,32},{1,49},{17,1},{33,17},{49,33},{2,50}... | collective-permute-start | bytes 786440 | tf_op jit(solution)/shard_map/ppermute | solution.py:258
  115.2 6.8 %collective-permute-start.6 = (bf16[256,128]{1,0:T(8,128)(2,1)}, bf16[256,128]{1,0:T(8,128)(2,1)S(1)}, u32[]{:S(2)}, u32[]{:S(2)}) collective-permute-start(bf16[256,128]{1,0:T(8,128)(2,1)} %get-tuple-element.9.refs_0_), channel_id=1, source_target_pairs={{128,0},{256,128},{384,256},{129,1},{257,129},{385,257},{130,2},{2... | collective-permute-start | bytes 196616 | tf_op jit(solution)/shard_map/ppermute | solution.py:258
  116.5 9.1 %collective-permute-start.5 = (bf16[256,128]{1,0:T(8,128)(2,1)}, bf16[256,128]{1,0:T(8,128)(2,1)S(1)}, u32[]{:S(2)}, u32[]{:S(2)}) collective-permute-start(bf16[256,128]{1,0:T(8,128)(2,1)} %get-tuple-element.9.refs_0_), channel_id=1, source_target_pairs={{256,0},{384,128},{257,1},{385,129},{258,2},{386,130},{259,3},{387... | collective-permute-start | bytes 196616 | tf_op jit(solution)/shard_map/ppermute | solution.py:258
  122.0 8.1 %copy-start.15 = (bf16[256,128]{1,0:T(8,128)(2,1)}, bf16[256,128]{1,0:T(8,128)(2,1)S(1)}, u32[]{:S(2)}) copy-start(bf16[256,128]{1,0:T(8,128)(2,1)S(1)} %collective-permute-done.6.refs_2_) | copy-start | bytes 196612
  122.0 8.1 %collective-permute-start.4 = (bf16[256,128]{1,0:T(8,128)(2,1)}, bf16[256,128]{1,0:T(8,128)(2,1)S(1)}, u32[]{:S(2)}, u32[]{:S(2)}) collective-permute-start(bf16[256,128]{1,0:T(8,128)(2,1)} %get-tuple-element.9.refs_0_), channel_id=1, source_target_pairs={{384,0},{385,1},{386,2},{387,3},{388,4},{389,5},{390,6},{391,7},{3... | collective-permute-start | bytes 196616 | tf_op jit(solution)/shard_map/ppermute | solution.py:258
  125.6 4.5 %copy-start.16 = (bf16[256,128]{1,0:T(8,128)(2,1)}, bf16[256,128]{1,0:T(8,128)(2,1)S(1)}, u32[]{:S(2)}) copy-start(bf16[256,128]{1,0:T(8,128)(2,1)S(1)} %collective-permute-done.5.refs_1_) | copy-start | bytes 196612
  130.1 0.8 copy-start.5
  130.1 0.9 copy-start.6
  138.4 8.0 %collective-permute-start.7 = (bf16[264,256]{1,0:T(8,128)(2,1)}, bf16[264,256]{1,0:T(8,128)(2,1)S(1)}, u32[]{:S(2)}, u32[]{:S(2)}) collective-permute-start(bf16[264,256]{1,0:T(8,128)(2,1)} %get-tuple-element.11), channel_id=1, source_target_pairs={{0,128},{128,256},{256,384},{1,129},{129,257},{257,385},{2,130},{1... | collective-permute-start | bytes 405512 | tf_op jit(solution)/shard_map/ppermute | solution.py:258
  139.7 6.7 %collective-permute-start.8 = (bf16[264,256]{1,0:T(8,128)(2,1)}, bf16[264,256]{1,0:T(8,128)(2,1)S(1)}, u32[]{:S(2)}, u32[]{:S(2)}) collective-permute-start(bf16[264,256]{1,0:T(8,128)(2,1)} %get-tuple-element.12), channel_id=1, source_target_pairs={{0,256},{128,384},{1,257},{129,385},{2,258},{130,386},{3,259},{131... | collective-permute-start | bytes 405512 | tf_op jit(solution)/shard_map/ppermute | solution.py:258
  141.0 5.5 %collective-permute-start.9 = (bf16[264,256]{1,0:T(8,128)(2,1)}, bf16[264,256]{1,0:T(8,128)(2,1)S(1)}, u32[]{:S(2)}, u32[]{:S(2)}) collective-permute-start(bf16[264,256]{1,0:T(8,128)(2,1)} %get-tuple-element.13), channel_id=1, source_target_pairs={{0,384},{1,385},{2,386},{3,387},{4,388},{5,389},{6,390},{7,391},{8... | collective-permute-start | bytes 405512 | tf_op jit(solution)/shard_map/ppermute | solution.py:258
  142.9 19.2 %copy-start.9 = (bf16[2048,128]{1,0:T(8,128)(2,1)S(1)}, bf16[2048,128]{1,0:T(8,128)(2,1)}, u32[]{:S(2)}) copy-start(bf16[2048,128]{1,0:T(8,128)(2,1)} %own_ref.1) | copy-start | bytes 1572868
  146.4 0.7 copy-start.13
  146.5 0.7 copy-start.14
  149.6 14.8 %copy-start.2 = (bf16[4,4,192,128]{3,2,1,0:T(8,128)(2,1)}, bf16[4,4,192,128]{3,2,1,0:T(8,128)(2,1)S(1)}, u32[]{:S(2)}) copy-start(bf16[4,4,192,128]{3,2,1,0:T(8,128)(2,1)S(1)} %all-to-all-done.2.hidden_ref) | copy-start | bytes 2359300
  149.6 29.8 %all-to-all-start = ((bf16[16,128,128]{2,1,0:T(8,128)(2,1)}), bf16[16,128,128]{2,1,0:T(8,128)(2,1)S(1)}, u32[]{:S(2)}, u32[]{:S(2)}) async-start(bf16[16,128,128]{2,1,0:T(8,128)(2,1)} %shard_map.179), calls=%async_computation | async-start | bytes 1048576 | tf_op jit(solution)/shard_map/all_to_all | solution.py:249
  162.1 24.3 %collective-permute-start.10 = (bf16[2048,128]{1,0:T(8,128)(2,1)S(1)}, bf16[2048,128]{1,0:T(8,128)(2,1)S(1)}, u32[]{:S(2)}, u32[]{:S(2)}) collective-permute-start(bf16[2048,128]{1,0:T(8,128)(2,1)S(1)} %copy-done.9), channel_id=1, source_target_pairs={{0,1},{1,0},{2,3},{3,2},{4,5},{5,4},{6,7},{7,6},{8,9},{9,8},{10,11... | collective-permute-start | bytes 1572872 | tf_op jit(solution)/shard_map/ppermute | solution.py:253
  179.3 7.1 %copy-start.3 = (bf16[16,128,128]{2,1,0:T(8,128)(2,1)}, bf16[16,128,128]{2,1,0:T(8,128)(2,1)S(1)}, u32[]{:S(2)}) copy-start(bf16[16,128,128]{2,1,0:T(8,128)(2,1)S(1)} %all-to-all-done.rows_ref) | copy-start | bytes 1572868
  179.3 20.8 %all-to-all-start.3 = ((bf16[128,8,128]{2,1,0:T(8,128)(2,1)}), bf16[128,8,128]{2,1,0:T(8,128)(2,1)S(1)}, u32[]{:S(2)}, u32[]{:S(2)}) async-start(bf16[128,8,128]{2,1,0:T(8,128)(2,1)} %bitcast.8), calls=%async_computation.3 | async-start | bytes 524288 | tf_op jit(solution)/shard_map/all_to_all | solution.py:249
  186.5 0.8 copy-start.10
  189.6 3.8 %collective-permute-start.11 = (bf16[128,128]{1,0:T(8,128)(2,1)}, bf16[128,128]{1,0:T(8,128)(2,1)S(1)}, u32[]{:S(2)}, u32[]{:S(2)}) collective-permute-start(bf16[128,128]{1,0:T(8,128)(2,1)} %get-tuple-element.15), channel_id=1, source_target_pairs={{0,1},{1,0},{2,3},{3,2},{4,5},{5,4},{6,7},{7,6},{8,9},{9,8},{10,11... | collective-permute-start | bytes 98312 | tf_op jit(solution)/shard_map/ppermute | solution.py:253
  (5 other events, 3.3 us)
